TPU v7x, 128 devices: a whole 4x4x4 slice. The times are simulated.
128 devices in a mesh: sp: 16 (over z, y), dp: 8 (over x, core).
Axes of the slice: x: 4, y: 4, z: 4, core: 2. Of those that a mesh axis runs over, the one named last changes fastest.
Arguments:
- tokens: bfloat16 [8, 8192, 2048], P('dp', 'sp'), may hold values from -6 to 6
- norm_gain: float32 [2048], replicated, may hold values from 0.1 to 1.9
- w_query: bfloat16 [2048, 1024], P(('sp', 'dp')), may hold values from -0.125 to 0.125
- w_key: bfloat16 [2048, 1024], P(('sp', 'dp')), may hold values from -0.125 to 0.125
- w_value: bfloat16 [2048, 2048], P(('sp', 'dp')), may hold values from -0.125 to 0.125
- w_out: bfloat16 [2048, 2048], P(('sp', 'dp')), may hold values from -0.125 to 0.125
- decay_rate: float32 [8, 8, 64], P('dp'), may hold values from 6.1035156e-06 to 0.08, as said below
Outputs:
- layer_out: bfloat16 [8, 8192, 2048], P('dp', 'sp')
Inputs may be any that keep to these rules, and one draw needn't show every extreme that they name: `decay_rate`: one rate for each sequence, head and block of 128 positions.
All inputs are finite; a program needn't handle non-finite values.
Results may differ from a plain program's by a relative error of at most 0.02.
Values may be sent and summed in bfloat16 or wider, within the bound.
A program may use at most 128 MiB of HBM per device.

v0:
```python
import jax
import jax.numpy as jnp
from jax import lax
from jax.sharding import Mesh
from jax.sharding import PartitionSpec as P

HEADS = 8
DK = 128
DV = 256
GROUP_W = 128
BLOCK = 128
SP = ("sp_0", "sp_1")
SP_DP = ("sp_0", "sp_1", "dp_0", "dp_1")
DP = ("dp_0", "dp_1")


EPS_RMS = 1e-06
EPS_GROUP = 0.01
ROPE_BASE = 10000.0


def filled_with(x, identity):
    return jax.tree.map(
        lambda part, zero: jnp.zeros_like(part) + jnp.asarray(zero, part.dtype), x, identity
    )


def prefix_by_axis(x, axes, combine, identity):
    before = start = filled_with(x, identity)
    total = x
    for axis in reversed(axes):
        count, here = (lax.axis_size(axis), lax.axis_index(axis))
        pieces = jax.tree.map(
            lambda part, kind: lax.all_gather(part.astype(kind), axis),
            total,
            (jnp.bfloat16, jnp.bfloat16),
        )
        inside, total = (start, start)
        for k in range(count):
            passed = k < here
            total = combine(
                total, jax.tree.map(lambda part, own: part[k].astype(own.dtype), pieces, x)
            )
            inside = jax.tree.map(lambda new, old: jnp.where(passed, new, old), total, inside)
        before = combine(inside, before)
    return before


def in_one_piece(arrays, axis, dim, along):
    ends, at = ([], 0)
    for a in arrays[:-1]:
        at += a.shape[along]
        ends.append(at)
    both = jnp.concatenate(arrays, axis=along)
    return tuple(jnp.split(lax.all_gather(both, axis, axis=dim, tiled=True), ends, axis=along))


def laid_out(parts, dim):
    parts = jnp.moveaxis(parts, 0, dim)
    shape = parts.shape
    return parts.reshape(*shape[:dim], shape[dim] * shape[dim + 1], *shape[dim + 2 :])


def gather_in_order(x, axes, turns):
    parts = x
    for k in turns:
        parts = lax.all_gather(parts, axes[k])
    done = turns[::-1]
    back = [done.index(k) for k in range(len(axes))]
    parts = parts.transpose(*back, *range(len(axes), parts.ndim))
    return parts.reshape(-1, *x.shape)


def gather_axes(x, axes, turns, dim):
    return laid_out(gather_in_order(x, axes, turns), dim)


def rms_scaled(token_rows, norm_gain):
    widened = token_rows.astype(jnp.float32)
    inv_norm = lax.rsqrt(jnp.mean(widened * widened, axis=-1, keepdims=True) + EPS_RMS)
    return (widened * inv_norm * norm_gain).astype(jnp.bfloat16)


def rope_tables(length, head_depth, first_pos):
    half_depth = head_depth // 2
    inverse = ROPE_BASE ** (-(jnp.arange(half_depth, dtype=jnp.float32) / (half_depth - 1)))
    places = first_pos.astype(jnp.float32) + jnp.arange(length, dtype=jnp.float32)
    angles = places[:, None] * inverse[None, :]
    return (jnp.cos(angles), jnp.sin(angles))


def rotate(stacked, cosine_table, sine_table):
    paired = stacked.reshape(stacked.shape[0], stacked.shape[1], -1, 2)
    first_part = paired[..., 0]
    second_part = paired[..., 1]
    cos_rows = cosine_table[:, None, :]
    sin_rows = sine_table[:, None, :]
    turned = jnp.stack(
        [
            first_part * cos_rows - second_part * sin_rows,
            second_part * cos_rows + first_part * sin_rows,
        ],
        axis=-1,
    )
    return turned.reshape(stacked.shape)


def combine_pairs(earlier, later):
    return (earlier[0] * later[0], later[0][..., None, None] * earlier[1] + later[1])


def from_earlier(last_decay, last_state):
    _, incoming = prefix_by_axis(
        (last_decay, last_state),
        SP,
        combine_pairs,
        (jnp.ones_like(last_decay), jnp.zeros_like(last_state)),
    )
    return incoming


def retain(queries, keys_in, values_in, decay_rows, carry_in):
    length, groups, head_depth = queries.shape
    blocks = length // BLOCK

    def by_block(stacked):
        return stacked.reshape(blocks, BLOCK, groups, stacked.shape[-1]).transpose(2, 0, 1, 3)

    query_blocks = by_block(queries)
    key_blocks = by_block(keys_in)
    value_blocks = by_block(values_in)
    offsets = jnp.arange(BLOCK, dtype=jnp.float32)
    distance = offsets[:, None] - offsets[None, :]
    within = jnp.where(
        distance >= 0.0, jnp.exp(-decay_rows[:, :, None, None] * jnp.maximum(distance, 0.0)), 0.0
    )
    scores = jnp.einsum(
        "gncd,gnmd->gncm", query_blocks, key_blocks, preferred_element_type=jnp.float32
    )
    weighted = (scores * within).astype(jnp.bfloat16)
    inner_sum = jnp.einsum(
        "gncm,gnme->gnce", weighted, value_blocks, preferred_element_type=jnp.float32
    )
    to_end = jnp.exp(-decay_rows[:, :, None] * (BLOCK - 1.0 - offsets))
    key_scaled = (key_blocks.astype(jnp.float32) * to_end[..., None]).astype(jnp.bfloat16)
    local_state = jnp.einsum(
        "gncd,gnce->gnde", key_scaled, value_blocks, preferred_element_type=jnp.float32
    )
    carried = jnp.exp(-decay_rows * BLOCK)
    cum_decay, cum_state = lax.associative_scan(combine_pairs, (carried, local_state), axis=1)
    incoming = carry_in(cum_decay[:, -1], cum_state[:, -1])
    before_local = jnp.concatenate([jnp.zeros_like(cum_state[:, :1]), cum_state[:, :-1]], axis=1)
    decay_before = jnp.concatenate([jnp.ones_like(cum_decay[:, :1]), cum_decay[:, :-1]], axis=1)
    before = before_local + decay_before[..., None, None] * incoming[:, None]
    from_start = jnp.exp(-decay_rows[:, :, None] * (offsets + 1.0))
    cross_term = jnp.einsum(
        "gncd,gnde->gnce", query_blocks.astype(jnp.float32) * from_start[..., None], before
    )
    mixed = inner_sum + cross_term
    return mixed.transpose(1, 2, 0, 3).reshape(length, groups, values_in.shape[-1])


def row_adder(left):

    def add_rows(running_sum, weight_piece, row_start):
        return jnp.dot(left, weight_piece, preferred_element_type=jnp.float32)

    return add_rows


def body(tokens, norm_gain, w_query, w_key, w_value, w_out, decay_rate):
    token_rows = tokens[0]
    local_count = token_rows.shape[0]
    normed_in = rms_scaled(token_rows, norm_gain)
    add_rows = row_adder(normed_in)
    query_empty = jnp.zeros((local_count, w_query.shape[1]), jnp.float32)
    value_empty = jnp.zeros((local_count, w_value.shape[1]), jnp.float32)
    out_empty = jnp.zeros((local_count, w_out.shape[1]), jnp.float32)
    pieces = in_one_piece((w_query, w_key, w_value), SP_DP, 0, 1)
    row_start = jnp.int32(0)
    query_sum = add_rows(query_empty, pieces[0], row_start)
    key_sum = add_rows(query_empty, pieces[1], row_start)
    value_sum = add_rows(value_empty, pieces[2], row_start)
    shard_index = lax.axis_index(SP)
    cosine_table, sine_table = rope_tables(local_count, DK, shard_index * local_count)
    query_rot = rotate(
        query_sum.astype(jnp.bfloat16).astype(jnp.float32).reshape(local_count, HEADS, DK),
        cosine_table,
        sine_table,
    ).astype(jnp.bfloat16)
    key_rot = (
        rotate(
            key_sum.astype(jnp.bfloat16).astype(jnp.float32).reshape(local_count, HEADS, DK),
            cosine_table,
            sine_table,
        )
        * DK ** (-0.5)
    ).astype(jnp.bfloat16)
    value_groups = value_sum.astype(jnp.bfloat16).reshape(local_count, 2 * HEADS, GROUP_W)
    blocks_here = local_count // BLOCK
    own_rates = lax.dynamic_slice_in_dim(decay_rate[0], shard_index * blocks_here, blocks_here, 1)
    mixed = retain(
        jnp.concatenate([query_rot, query_rot], axis=1),
        jnp.concatenate([key_rot, key_rot], axis=1),
        value_groups,
        jnp.concatenate([own_rates, own_rates], axis=0),
        from_earlier,
    )
    halves = mixed.reshape(local_count, 2, HEADS, GROUP_W)
    mean_part = jnp.sum(halves, axis=(1, 3), keepdims=True) / DV
    square_part = jnp.sum(halves * halves, axis=(1, 3), keepdims=True) / DV
    retained = (
        ((halves - mean_part) * lax.rsqrt(square_part - mean_part * mean_part + EPS_GROUP))
        .astype(jnp.bfloat16)
        .reshape(local_count, -1)
    )
    result = row_adder(retained)(
        out_empty, gather_axes(w_out, (("sp_0", "sp_1", "dp_0"), "dp_1"), (0, 1), 0), jnp.int32(0)
    )
    return result.astype(jnp.bfloat16)[None]


def solution(mesh):
    split = Mesh(mesh.devices.reshape(4, 4, 4, 2), ("sp_0", "sp_1", "dp_0", "dp_1"))
    in_specs = (
        P(DP, SP, None),
        P(),
        P(SP_DP, None),
        P(SP_DP, None),
        P(SP_DP, None),
        P(SP_DP, None),
        P(DP, None, None),
    )
    out_specs = P(DP, SP, None)
    return jax.shard_map(body, mesh=split, in_specs=in_specs, out_specs=out_specs, check_vma=False)
```

profile of v0, /device:TPU:1, one launch (start us, length us, event | category | flops | bytes accessed | tf_op | source)
XLA Modules:
  0.0 301.4 jit_solution(13576277298096494629)
XLA Ops:
  9.6 2.1 fusion.2
  12.3 81.8 %all-gather.11.cloned.1.call-done = bf16[2048,4096]{1,0:T(8,128)(2,1)} async-done(((bf16[16,4096]{1,0:T(8,128)(2,1)}), bf16[2048,4096]{1,0:T(8,128)(2,1)}) %all-gather.11.cloned.1.call-update) | async-done | bytes 16777232 | tf_op jit(solution)/shard_map/all_gather | solution.py:55
  94.1 5.9 %fusion.36 = f32[512,1024]{1,0:T(8,128)} fusion(bf16[2048,4096]{1,0:T(8,128)(2,1)} %all-gather.11.cloned.1.call-done, bf16[1,512,2048]{2,1,0:T(8,128)(2,1)S(1)} %copy-done.7, f32[2048]{0:T(1024)S(1)} %copy-done.10, f32[512]{0:T(512)S(1)} %add_rsqrt_fusion.1), kind=kOutput, calls=%fused_computation.48 | convolution fusion | flops 2152726528 | bytes 8398848 | tf_op jit(solution)/shard_map/dot_general | solution.py:166
  100.0 1.9 copy.74
  101.9 2.2 reshape.374
  104.2 6.6 %fusion.42 = f32[512,1024]{1,0:T(8,128)} fusion(bf16[2048,4096]{1,0:T(8,128)(2,1)} %all-gather.11.cloned.1.call-done, bf16[1,512,2048]{2,1,0:T(8,128)(2,1)} %param.7, f32[2048]{0:T(1024)S(1)} %copy-done.10, f32[512]{0:T(512)S(1)} %add_rsqrt_fusion.1), kind=kOutput, calls=%fused_computation.50 | convolution fusion | flops 2152726528 | bytes 8398848 | tf_op jit(solution)/shard_map/dot_general | solution.py:166
  110.7 1.9 copy.80
  112.7 2.2 reshape.375
  114.9 7.9 %fusion.94 = (f32[512,8,64,1]{0,3,2,1:T(1,128)S(1)}, f32[512,8,64,1]{0,3,2,1:T(1,128)S(1)}, f32[512,8,64,1]{0,3,2,1:T(1,128)S(1)}, f32[512,8,64,1]{0,3,2,1:T(1,128)S(1)}) fusion(f32[512,8,64,2]{0,3,2,1:T(2,128)} %reshape.374, f32[512,8,64,2]{0,3,2,1:T(2,128)} %reshape.375), kind=kLoop, calls=%fused_computation.156 | loop fusion | bytes 8388608 | tf_op jit(solution)/shard_map/slice | solution.py:94
  122.8 1.7 subtract_convert_fusion
  126.8 8.9 %fusion.30 = bf16[64,8,16,128]{3,1,2,0:T(8,128)(2,1)S(1)} fusion(bf16[2048,4096]{1,0:T(8,128)(2,1)} %all-gather.11.cloned.1.call-done, bf16[1,512,2048]{2,1,0:T(8,128)(2,1)} %param.7, f32[2048]{0:T(1024)S(1)} %copy-done.10, f32[512]{0:T(512)S(1)} %add_rsqrt_fusion.1), kind=kOutput, calls=%fused_computation.46 | convolution fusion | flops 4300210176 | bytes 12593152 | tf_op jit(solution)/shard_map/dot_general | solution.py:166
  136.4 3.3 %fusion.20 = f32[16,4,128,128]{3,2,1,0:T(8,128)S(1)} fusion(f32[16,4,128]{2,1,0:T(4,128)S(1)} %get-tuple-element.26, bf16[4,128,8,128]{3,1,0,2:T(8,128)(2,1)S(1)} %copy.84, bf16[4,128,16,128]{3,2,1,0:T(8,128)(2,1)S(1)} %bitcast.210), kind=kOutput, calls=%fused_computation.31 | convolution fusion | flops 272629760 | bytes 7372800 | tf_op jit(solution)/shard_map/gncd,gnce->gnde/dot_general | solution.py:146
  143.1 11.8 %pad.117 = f32[16,3,128,128]{3,2,1,0:T(8,128)} pad(f32[16,2,128,128]{3,2,1,0:T(8,128)S(1)} %pad_add_fusion, f32[]{:T(128)} %constant.20.clone.1), padding=0_0_0x0_0_1x0_0_0x0_0_0 | pad | bytes 5242884
  154.8 2.2 add_convert_fusion
  157.1 6.4 %all-gather.17.cloned.1.call-done = bf16[1024,2048]{1,0:T(8,128)(2,1)} async-done(((bf16[16,2048]{1,0:T(8,128)(2,1)}), bf16[1024,2048]{1,0:T(8,128)(2,1)}) %all-gather.17.cloned.1.call-update) | async-done | bytes 4194320 | tf_op jit(solution)/shard_map/all_gather | solution.py:67
  165.7 7.6 %all-reduce.10 = bf16[64]{0:T(256)(128)(2,1)S(1)} all-reduce(bf16[64]{0:T(256)(128)(2,1)S(1)} %dynamic-update-slice), channel_id=2, replica_groups=mesh['sp_0'=4,'sp_1'=4,'dp_0'=4,'dp_1'=2] {'sp_1'}, use_global_device_ids=true, to_apply=%add.10 | all-reduce | flops 64 | bytes 256
  173.4 20.9 %all-gather.15.cloned.1.call-done = bf16[64,1,128,128]{3,2,1,0:T(8,128)(2,1)} async-done(((bf16[16,1,128,128]{3,2,1,0:T(8,128)(2,1)}), bf16[64,1,128,128]{3,2,1,0:T(8,128)(2,1)}) %all-gather.15.cloned.1.call-update) | async-done | bytes 2097168 | tf_op jit(solution)/shard_map/all_gather | solution.py:34
  194.3 2.9 fusion.52
  197.3 7.9 %all-gather.4 = bf16[4,1,16]{2,1,0:T(2,128)(2,1)S(1)} all-gather(bf16[1,1,16]{2,1,0:T(2,128)(2,1)S(1)} %fusion.81), channel_id=1, replica_groups=mesh['sp_0'=4,'sp_1'=4,'dp_0'=4,'dp_1'=2] {'sp_0'}, dimensions={0}, use_global_device_ids=true | all-gather | bytes 160 | tf_op jit(solution)/shard_map/all_gather | solution.py:34
  205.5 13.6 %all-gather.19.cloned.1.call-done = bf16[128,16,2048]{2,1,0:T(8,128)(2,1)} async-done(((bf16[64,16,2048]{2,1,0:T(8,128)(2,1)}), bf16[128,16,2048]{2,1,0:T(8,128)(2,1)}) %all-gather.19.cloned.1.call-update) | async-done | bytes 8388624 | tf_op jit(solution)/shard_map/all_gather | solution.py:67
  219.0 8.4 %copy.97 = bf16[64,2,16,2048]{3,2,1,0:T(8,128)(2,1)} copy(bf16[64,2,16,2048]{3,2,0,1:T(8,128)(2,1)} %bitcast.212) | data formatting | bytes 16777216 | tf_op jit(solution)/shard_map/transpose | solution.py:70
  227.5 12.0 %pad.31 = f32[16,4,128,128]{3,2,1,0:T(8,128)} pad(f32[16,2,128,128]{3,2,1,0:T(8,128)S(1)} %pad_add_fusion, f32[]{:T(128)} %constant.20.clone.1), padding=0_0_0x1_0_1x0_0_0x0_0_0 | pad | bytes 6291460 | tf_op jit(solution)/shard_map/pad | solution.py:150
  239.5 2.1 fusion.93
  241.8 12.0 %pad.30 = f32[16,4,128,128]{3,2,1,0:T(8,128)} pad(f32[16,2,128,128]{3,2,1,0:T(8,128)S(1)} %pad_maximum_fusion, f32[]{:T(128)} %constant.20.clone.1), padding=0_0_0x0_1_1x0_0_0x0_0_0 | pad | bytes 6291460 | tf_op jit(solution)/shard_map/pad | solution.py:150
  254.8 1.7 copy.78
  256.5 3.3 %slice_add_fusion = f32[16,3,128,128]{3,2,1,0:T(8,128)S(1)} fusion(f32[16,4,128,128]{3,2,1,0:T(8,128)} %pad.31, f32[16,4,128,128]{3,2,1,0:T(8,128)} %pad.30), kind=kLoop, calls=%fused_computation.23 | loop fusion | flops 786432 | bytes 9437184 | tf_op jit(solution)/shard_map/add | solution.py:150
  259.9 4.5 %fusion.60 = f32[16,128,128]{2,1,0:T(8,128)S(1)} fusion(bf16[4,16,128,128]{3,2,1,0:T(8,128)(2,1)} %all-gather.13.cloned.1.call-done, f32[16]{0:T(128)S(1)} %get-tuple-element.41, f32[16]{0:T(128)S(1)} %get-tuple-element.44, f32[16]{0:T(128)S(1)} %get-tuple-element.43, f32[16]{0:T(128)S(1)} %get-tuple-element.42, f32[16]{0:T(128)S(1)} %fusion.76, ...), kind=kLoop, calls=%fused_computation.74 | loop fusion | flops 8388608 | bytes 5243464 | tf_op jit(solution)/shard_map/add | solution.py:109
  264.4 3.6 %fusion.10 = f32[16,4,128,128]{3,2,1,0:T(8,128)} fusion(f32[16,3,128,128]{3,2,1,0:T(8,128)S(1)} %slice_add_fusion, f32[16,128,128]{2,1,0:T(8,128)S(1)} %fusion.60, f32[16,4]{1,0:T(8,128)S(1)} %concatenate.44.clone, f32[16,4,128]{2,1,0:T(4,128)S(1)} %get-tuple-element.25, bf16[4,128,8,128]{3,1,0,2:T(8,128)(2,1)S(1)} %copy-done.6), kind=kOutput, calls=%fused_computation.15 | convolution fusion | flops 273678336 | bytes 9470208 | tf_op jit(solution)/shard_map/gncd,gnde->gnce/dot_general | solution.py:156
  267.9 9.5 %bitcast_reduce_fusion = (f32[4,128,16]{1,0,2:T(4,128)S(1)}, f32[4,128,16]{1,0,2:T(4,128)S(1)}, f32[16,4,128,128]{3,2,1,0:T(8,128)}) fusion(f32[16,4,128,128]{3,2,1,0:T(8,128)} %fusion.10, bf16[4,128,16,128]{3,2,1,0:T(8,128)(2,1)} %bitcast.211, f32[128,128]{1,0:T(8,128)S(1)} %fusion.73, f32[16,4]{1,0:T(8,128)S(1)} %copy.87, ...), kind=kOutput, calls=%fused_computation.11 | convolution fusion | flops 547340288 | bytes 12730624 | tf_op jit(solution)/shard_map/gncm,gnme->gnce/dot_general | solution.py:141
  277.4 5.4 %copy.96 = f32[512,2,8,128]{0,3,2,1:T(8,128)} copy(f32[512,2,8,128]{3,0,2,1:T(8,128)} %bitcast.217) | data formatting | bytes 8388608 | tf_op jit(solution)/shard_map/reshape;reshape | solution.py:209
  282.8 2.9 multiply_convert_fusion
  285.7 9.1 %fusion.19 = bf16[1,512,2048]{2,1,0:T(8,128)(2,1)} fusion(bf16[512,2048]{0,1:T(8,128)(2,1)S(1)} %bitcast.218, bf16[2048,2048]{1,0:T(8,128)(2,1)} %bitcast.213), kind=kOutput, calls=%fused_computation.26 | convolution fusion | flops 4296015872 | bytes 12582912 | tf_op jit(solution)/shard_map/dot_general | solution.py:166
  (87 shorter events, 13.0 us)
Async XLA Ops:
  6.5 2.5 copy-start
  6.5 87.5 %copy-start.7 = (bf16[1,512,2048]{2,1,0:T(8,128)(2,1)S(1)}, bf16[1,512,2048]{2,1,0:T(8,128)(2,1)}, u32[]{:S(2)}) copy-start(bf16[1,512,2048]{2,1,0:T(8,128)(2,1)} %param.7) | copy-start | bytes 6291460
  6.5 87.5 %copy-start.10 = (f32[2048]{0:T(1024)S(1)}, f32[2048]{0:T(1024)}, u32[]{:S(2)}) copy-start(f32[2048]{0:T(1024)} %param.8) | copy-start | bytes 24580
  6.5 87.5 %all-gather.11.cloned.1.call-start = ((), (), s32[]{:S(2)}) async-start(), calls=%async_computation | async-start | bytes 16908288 | tf_op jit(solution)/shard_map/all_gather | solution.py:55
  8.2 155.2 %all-gather.17.cloned.1.call-start = ((), (), s32[]{:S(2)}) async-start(), calls=%async_computation.3 | async-start | bytes 4259840 | tf_op jit(solution)/shard_map/all_gather | solution.py:67
  9.0 185.4 %all-gather.15.cloned.1.call-start = ((), (), s32[]{:S(2)}) async-start(), calls=%async_computation.2 | async-start | bytes 2621440 | tf_op jit(solution)/shard_map/all_gather | solution.py:34
  126.7 9.6 %copy-start.5 = (bf16[4,128,8,128]{3,1,0,2:T(8,128)(2,1)}, bf16[4,128,8,128]{3,1,0,2:T(8,128)(2,1)S(1)}, u32[]{:S(2)}) copy-start(bf16[4,128,8,128]{3,1,0,2:T(8,128)(2,1)S(1)} %copy.84) | copy-start | bytes 3145732
  136.3 3.3 %copy-start.4 = (bf16[64,8,16,128]{3,2,1,0:T(8,128)(2,1)}, bf16[64,8,16,128]{3,2,1,0:T(8,128)(2,1)S(1)}, u32[]{:S(2)}) copy-start(bf16[64,8,16,128]{3,2,1,0:T(8,128)(2,1)S(1)} %copy.104) | copy-start | bytes 6291460
  139.7 1.9 copy-start.2
  141.8 1.0 copy-start.3
  157.0 62.0 %all-gather.19.cloned.1.call-start = ((), (), s32[]{:S(2)}) async-start(), calls=%async_computation.4 | async-start | bytes 12582912 | tf_op jit(solution)/shard_map/all_gather | solution.py:67
  163.5 0.7 copy-start.11
  163.5 96.4 %all-gather.13.cloned.1.call-start = ((), (), s32[]{:S(2)}) async-start(), calls=%async_computation.1 | async-start | bytes 2621440 | tf_op jit(solution)/shard_map/all_gather | solution.py:34
  241.8 12.0 %copy-start.8 = (bf16[512,8,64,1]{0,2,3,1:T(8,128)(2,1)S(1)}, bf16[512,8,64,1]{0,2,3,1:T(8,128)(2,1)}, u32[]{:S(2)}) copy-start(bf16[512,8,64,1]{0,2,3,1:T(8,128)(2,1)} %get-tuple-element.11) | copy-start | bytes 1572868
  241.8 12.0 %copy-start.9 = (bf16[512,8,64,1]{0,2,3,1:T(8,128)(2,1)S(1)}, bf16[512,8,64,1]{0,2,3,1:T(8,128)(2,1)}, u32[]{:S(2)}) copy-start(bf16[512,8,64,1]{0,2,3,1:T(8,128)(2,1)} %get-tuple-element.12) | copy-start | bytes 1572868
  259.9 4.5 %copy-start.6 = (bf16[4,128,8,128]{3,1,0,2:T(8,128)(2,1)S(1)}, bf16[4,128,8,128]{3,1,0,2:T(8,128)(2,1)}, u32[]{:S(2)}) copy-start(bf16[4,128,8,128]{3,1,0,2:T(8,128)(2,1)} %copy.78) | copy-start | bytes 3145732
  285.7 9.2 %copy-start.1 = (f32[1,8,64]{2,1,0:T(8,128)S(1)}, f32[1,8,64]{2,1,0:T(8,128)}, u32[]{:S(2)}) copy-start(f32[1,8,64]{2,1,0:T(8,128)} %param.13) | copy-start | bytes 6148
Sparse Core Ops, SparseCore 0:
  10.5 83.5 all-gather.10
  97.0 66.4 all-gather.16
  165.1 29.1 all-gather.14
  195.8 23.1 all-gather.18
  220.5 31.7 all-gather.12
where the time goes:
time: 302 us; the launch traced here: 301 us
  waiting for transfers between devices  123 us (41%)
  local copies, waits for them, and re-layouts  75.6 us (25%)
  matrix products  46.9 us (16%)
  other arithmetic  25.6 us (8%)
  blocking collectives  15.5 us (5%)
  between operations  14.2 us (5%)
    all_gather x1, waiting for transfers between devices, in_one_piece(): lax.all_gather(both, axis, axis=dim, tiled=True)  81.8 us
    dot_general x4, matrix products, add_rows(): return jnp.dot(left, weight_piece, preferred_element_type=jnp.float32)  30.6 us
    pad x4, local copies, waits for them, and re-layouts, retain(): lax.associative_scan(combine_pairs, (carried, local_state), axis=1)  24 us
    all_gather x2, waiting for transfers between devices, prefix_by_axis(): lax.all_gather(part.astype(kind), axis)  20.9 us
    all_gather x2, waiting for transfers between devices, gather_in_order(): parts = lax.all_gather(parts, axes[k])  20 us
    unnamed x31, local copies, waits for them, and re-layouts  16.6 us
    dot_general x1, matrix products, retain(): jnp.einsum('gncm,gnme->gnce', weighted, value_blocks, preferred_element_t...  9.46 us
    transpose x1, local copies, waits for them, and re-layouts, gather_in_order(): parts = parts.transpose(*back, *range(len(axes), parts.ndim))  8.44 us
  transfers between devices with their start and end apart: 5, of which 4 were waited for; matrix products, arithmetic and copies ran while one was open for 36% of the time, Pallas kernels for 0%

commit v1 on v0

v1 whole, which is shorter than its diff:
```python
import functools

import jax
import jax.numpy as jnp
import numpy as np
from jax import lax
from jax.experimental import pallas as pl
from jax.experimental.pallas import tpu as pltpu
from jax.sharding import Mesh
from jax.sharding import PartitionSpec as P

MESH = pl.DeviceIdType.MESH
F32 = jnp.float32
BF16 = jnp.bfloat16

HEADS = 8
DK = 128
DV = 256
BLOCK = 128
D = 2048
LEN = 512
SHARDS = 16
EPS_RMS = 1e-06
EPS_GROUP = 0.01
ROPE_BASE = 10000.0

K_PIECES = (0, 3)
V_PIECES = (1, 2, 4, 5)
Q_PIECES = (6, 7)
O_FIRST = 8
WAVES = 4
ORDERS = ((2, 1, 0), (1, 0, 2), (0, 2, 1))


def rope_constants():
    inverse = ROPE_BASE ** (-(np.arange(DK // 2, dtype=np.float64) / (DK // 2 - 1)))
    inverse = np.repeat(inverse, 2)
    high = np.arange(256, dtype=np.float64)[:, None] * 32 * inverse[None, :]
    low = np.arange(32, dtype=np.float64)[:, None] * inverse[None, :]
    high = np.stack([np.cos(high), np.sin(high)]).astype(np.float32)
    low = np.stack([np.cos(low), np.sin(low)]).astype(np.float32)
    return high, low


def kernel(
    tokens, gain, wq, wk, wv, wo, rates, high, low,
    out,
    w, x_raw, xn, rates2, cos_t, sin_t, rate_b, base_b, dec,
    keys, queries, values, s_send, s_recv, p_send, p_recv, ret, ret_send, out_v,
    tok_sem, own_sem, mate_s, mate_r, rate_s, rate_r, xn_s, xn_r,
    p1s, p1r, p2s, p2r, p2fs, p2fr, p3s, p3r, p3fs, p3fr,
    ss, sr, ps, pr, rs, rr, os, orr, out_sem,
):
    z, y, x, c = (lax.axis_index(a) for a in ("z", "y", "x", "c"))
    here = (z, y, x)
    shard = z * 4 + y
    mate = (z, y, x, 1 - c)

    def device(dim, step):
        at = list(here)
        at[dim] = lax.rem(at[dim] + step, 4)
        return (*at, c)

    def peer(step):
        to = lax.rem(shard + step, SHARDS)
        return to, (lax.div(to, 4), lax.rem(to, 4), x, c)

    tok_copies = []
    for i in range(4):
        rows = pl.ds(i * 128, 128)
        cp = pltpu.make_async_copy(tokens.at[0, rows], x_raw.at[rows], tok_sem.at[i])
        tok_copies.append(cp)

    def pieces_of(wave, core):
        todo = []
        for piece in range(3 * wave, 3 * wave + 3):
            if piece in K_PIECES or piece in Q_PIECES:
                ref = wk if piece in K_PIECES else wq
                j = K_PIECES.index(piece) if piece in K_PIECES else Q_PIECES.index(piece)
                at = pl.multiple_of(core * 512 + j * 256, 256)
                todo.append((ref.at[:, pl.ds(at, 256)], piece, pl.ds(0, 256)))
            elif piece in V_PIECES:
                h = V_PIECES.index(piece)
                for s in range(2):
                    at = pl.multiple_of(core * 512 + (s * 1024 + h * 128), 128)
                    todo.append((wv.at[:, pl.ds(at, 128)], piece, pl.ds(s * 128, 128)))
            else:
                at = pl.multiple_of(core * 1024 + (piece - O_FIRST) * 256, 256)
                todo.append((wo.at[:, pl.ds(at, 256)], piece, pl.ds(0, 256)))
        return todo

    own_rows = pl.ds(pl.multiple_of(c * 16, 16), 16)
    for wave in range(WAVES):
        for src, piece, cols in pieces_of(wave, c):
            pltpu.make_async_copy(src, w.at[piece, z, y, x, own_rows, cols], own_sem.at[wave]).start()
        if wave == 0:
            for cp in tok_copies:
                cp.start()

    barrier = pltpu.get_barrier_semaphore()

    def greet(step, carry):
        _, dev = peer(step)
        pl.semaphore_signal(barrier, inc=1, device_id=dev, device_id_type=MESH)
        return carry

    lax.fori_loop(1, SHARDS, greet, 0)
    for step in range(1, 4):
        pl.semaphore_signal(barrier, inc=1, device_id=device(2, step), device_id_type=MESH)
    pl.semaphore_signal(barrier, inc=1, device_id=mate, device_id_type=MESH)
    pl.semaphore_wait(barrier, 19)

    for wave in range(WAVES):
        for src, piece, cols in pieces_of(wave, 1 - c):
            pltpu.make_async_remote_copy(
                src, w.at[piece, z, y, x, own_rows, cols],
                mate_s.at[wave], mate_r.at[wave], device_id=mate, device_id_type=MESH,
            ).start()
        if wave == 0:
            rate_copy = pltpu.make_async_remote_copy(
                rates, rates2, rate_s, rate_r, device_id=mate, device_id_type=MESH
            )
            rate_copy.start()

    def part_slice(piece, where):
        idx = tuple(where.get(d, pl.ds(0, 4)) for d in range(3))
        return w.at[(piece, *idx)]

    def send(src, ssem, rsem, dev):
        pltpu.make_async_remote_copy(src, src, ssem, rsem, device_id=dev, device_id_type=MESH).start()

    def drain(ref, sem):
        pltpu.make_async_copy(ref, ref, sem).wait()

    def three(wave):
        return pl.ds(3 * wave, 3)

    def p1_wait_ref(wave):
        return w.at[three(wave), 0, 0, pl.ds(0, 3)]

    def p2_wait_ref(wave):
        return w.at[three(wave), pl.ds(0, 2), 0]

    def p2f_wait_ref(wave):
        return w.at[three(wave), 0, 0]

    def half_wait_ref(wave):
        return w.at[3 * wave, pl.ds(0, 2), 0]

    HALF = (pl.ds(0, 2), pl.ds(2, 2))

    def stage_p0(wave):
        ref = w.at[three(wave), 0, 0, 0, pl.ds(0, 16)]
        drain(ref, own_sem.at[wave])
        drain(ref, mate_r.at[wave])
        for part, (d1, d2, d3) in enumerate(ORDERS):
            piece = 3 * wave + part
            own = part_slice(piece, {0: z, 1: y, 2: x})
            for step in (1, 3, 2):
                send(own, p1s.at[wave], p1r.at[wave], device(d1, step))

    def stage_a(wave):
        drain(p1_wait_ref(wave), p1r.at[wave])
        for part, (d1, d2, d3) in enumerate(ORDERS):
            own = part_slice(3 * wave + part, {d2: here[d2], d3: here[d3]})
            for step in (1, 3):
                send(own, p2s.at[wave], p2r.at[wave], device(d2, step))

    def stage_b(wave):
        drain(p2_wait_ref(wave), p2r.at[wave])
        for part, (d1, d2, d3) in enumerate(ORDERS):
            for i, step in enumerate((1, 3)):
                origin = lax.rem(here[d2] + 4 - step, 4)
                src = part_slice(3 * wave + part, {d1: HALF[i], d2: origin, d3: here[d3]})
                send(src, p2fs.at[wave], p2fr.at[wave], device(d2, step))

    def stage_c(wave):
        drain(p2f_wait_ref(wave), p2fr.at[wave])
        for sub in range(2):
            for part, (d1, d2, d3) in enumerate(ORDERS):
                for i, step in enumerate((1, 3)):
                    half = sub if i == 0 else 1 - sub
                    src = part_slice(3 * wave + part, {d2: HALF[half], d3: here[d3]})
                    send(src, p3s.at[wave], p3r.at[wave, part, i, sub], device(d3, step))

    def stage_d(wave):
        for part, (d1, d2, d3) in enumerate(ORDERS):
            for i, step in enumerate((1, 3)):
                drain(half_wait_ref(wave), p3r.at[wave, part, i, 0])
                origin = lax.rem(here[d3] + 4 - step, 4)
                src = part_slice(3 * wave + part, {d2: HALF[i], d3: origin})
                send(src, p3fs.at[wave], p3fr.at[wave, part, i], device(d3, step))

    def stage_e(wave):
        for part in range(3):
            for i in range(2):
                drain(half_wait_ref(wave), p3r.at[wave, part, i, 1])
                drain(half_wait_ref(wave), p3fr.at[wave, part, i])

    def finish_sends(wave):
        drain(w.at[three(wave), 0, 0, 0, pl.ds(0, 16)], mate_s.at[wave])
        drain(p1_wait_ref(wave), p1s.at[wave])
        drain(p2_wait_ref(wave), p2s.at[wave])
        drain(p2f_wait_ref(wave), p2fs.at[wave])
        drain(w.at[three(wave), pl.ds(0, 2)], p3s.at[wave])
        drain(w.at[three(wave), 0], p3fs.at[wave])

    def norm(i):
        rows = pl.ds(i * 128, 128)
        tok_copies[i].wait()
        wide = x_raw[rows].astype(F32)
        inv = lax.rsqrt(jnp.sum(wide * wide, axis=-1, keepdims=True) * (1.0 / D) + EPS_RMS)
        xn[0, rows] = (wide * inv * gain[...]).astype(BF16)

    def norm_copy(i):
        rows = pl.ds(i * 128, 128)
        return pltpu.make_async_remote_copy(
            xn.at[0, rows], xn.at[1, rows], xn_s.at[i], xn_r.at[i], device_id=mate, device_id_type=MESH
        )

    def tables():
        lane = lax.broadcasted_iota(jnp.int32, (32, DK), 1)
        sign = jnp.where(lax.rem(lane, 2) == 0, -1.0, 1.0).astype(F32)
        cl, sl = low[0], low[1]
        for i in range(16):
            at = shard * 16 + i
            ch, sh = high[0, pl.ds(at, 1)], high[1, pl.ds(at, 1)]
            cos_t[pl.ds(i * 32, 32)] = ch * cl - sh * sl
            sin_t[pl.ds(i * 32, 32)] = (sh * cl + ch * sl) * sign

    def decays():
        lane = lax.broadcasted_iota(jnp.int32, (4, 64), 1)
        for s in range(2):
            full = rates[...] if s == 0 else rates2[...]
            mine = jnp.where(c == 0, full[0:4], full[4:8])
            base = jnp.zeros((4, 1), F32)
            for n in range(4):
                r = jnp.sum(jnp.where(lane == shard * 4 + n, mine, 0.0), axis=1, keepdims=True)
                rate_b[s, n] = jnp.broadcast_to(r, (4, 128))
                base_b[s, n] = jnp.broadcast_to(base, (4, 128))
                base = base + r * float(BLOCK)
            base_b[s, 4] = jnp.broadcast_to(base, (4, 128))
            for t in range(SHARDS - 1):
                tot = jnp.sum(jnp.where(lax.div(lane, 4) == t, mine, 0.0), axis=1, keepdims=True)
                e = jnp.broadcast_to(jnp.exp(tot * (-float(BLOCK))), (4, 128))
                for h in range(4):
                    dec[h // 2, s * 2 + h % 2, pl.ds(t, 1)] = e[h : h + 1]

    def turned(prod, s, h, sign, scale):
        v = prod.astype(BF16).astype(F32)
        even = lax.rem(lax.broadcasted_iota(jnp.int32, v.shape, 1), 2) == 0
        swap = jnp.where(even, pltpu.roll(v, DK - 1, 1), pltpu.roll(v, 1, 1))
        rot = v * cos_t[...] + swap * sin_t[...]
        offset = (lax.broadcasted_iota(jnp.int32, (BLOCK, DK), 0) + 1).astype(F32)
        parts = []
        for n in range(4):
            e = base_b[s, n, pl.ds(h, 1)] + rate_b[s, n, pl.ds(h, 1)] * offset
            parts.append(rot[n * BLOCK : (n + 1) * BLOCK] * (jnp.exp(e * sign) * scale))
        return jnp.concatenate(parts, axis=0).astype(BF16)

    def project(s, piece):
        return jnp.dot(xn[s], w[piece].reshape(D, 256), preferred_element_type=F32)

    def key_piece(j):
        def body(s, carry):
            prod = project(s, K_PIECES[j])
            for hh in range(2):
                h = 2 * j + hh
                keys[s, h] = turned(prod[:, hh * 128 : (hh + 1) * 128], s, h, 1.0, DK ** (-0.5))
            return carry
        lax.fori_loop(0, 2, body, 0)

    def query_piece(j):
        def body(s, carry):
            prod = project(s, Q_PIECES[j])
            for hh in range(2):
                h = 2 * j + hh
                queries[s, h] = turned(prod[:, hh * 128 : (hh + 1) * 128], s, h, -1.0, 1.0)
            return carry
        lax.fori_loop(0, 2, body, 0)

    def value_piece(h):
        def body(s, carry):
            values[s, h] = project(s, V_PIECES[h]).astype(BF16)
            return carry
        lax.fori_loop(0, 2, body, 0)

    def local_states(half):
        def body(p, carry):
            s, h = lax.div(p, 2), half * 2 + lax.rem(p, 2)
            st = lax.dot_general(
                keys[s, h], values[s, h], (((0,), (0,)), ((), ())), preferred_element_type=F32
            )
            e = jnp.exp(-base_b[s, 4, pl.ds(h, 1)])
            e = jnp.concatenate([e, e], axis=1)
            s_send[half, pl.ds(p * 4, 4)] = (st * e).astype(BF16).reshape(4, 32, DV)
            return carry
        lax.fori_loop(0, 4, body, 0)
        s_recv[half, shard] = s_send[half, shard]

    def send_states(half):
        def body(step, carry):
            to, dev = peer(step)
            pltpu.make_async_remote_copy(
                s_send.at[half, to], s_recv.at[half, shard], ss.at[half], sr.at[half],
                device_id=dev, device_id_type=MESH,
            ).start()
            return carry
        lax.fori_loop(1, SHARDS, body, 0)

    def scan_states(half):
        drain(s_recv.at[half, pl.ds(0, SHARDS - 1)], sr.at[half])
        run = jnp.zeros((32, DV), F32)
        rows = dec[half, z]
        for t in range(SHARDS):
            p_send[half, t] = run.astype(BF16)
            if t < SHARDS - 1:
                e = rows[t : t + 1]
                run = run * jnp.concatenate([e, e], axis=1) + s_recv[half, t].astype(F32)
        p_recv[half, shard] = p_send[half, shard]

    def send_prefixes(half):
        def body(step, carry):
            to, dev = peer(step)
            pltpu.make_async_remote_copy(
                p_send.at[half, to], p_recv.at[half, shard], ps.at[half], pr.at[half],
                device_id=dev, device_id_type=MESH,
            ).start()
            return carry
        lax.fori_loop(1, SHARDS, body, 0)

    def retention(s, half):
        row = lax.broadcasted_iota(jnp.int32, (256, 256), 0)
        col = lax.broadcasted_iota(jnp.int32, (256, 256), 1)
        def body(hh, carry):
            h = half * 2 + hh
            p = s * 2 + hh
            before = p_recv[half, pl.ds(p * 4, 4)].reshape(DK, DV)
            for i in range(2):
                q = queries[s, h, pl.ds(i * 256, 256)]
                mixed = jnp.dot(q, before, preferred_element_type=F32)
                for j in range(i + 1):
                    k = keys[s, h, pl.ds(j * 256, 256)]
                    sc = lax.dot_general(q, k, (((1,), (1,)), ((), ())), preferred_element_type=F32)
                    if i == j:
                        sc = jnp.where(row >= col, sc, 0.0)
                    mixed = mixed + jnp.dot(
                        sc.astype(BF16), values[s, h, pl.ds(j * 256, 256)], preferred_element_type=F32
                    )
                mu = jnp.sum(mixed, axis=1, keepdims=True) * (1.0 / DV)
                sq = jnp.sum(mixed * mixed, axis=1, keepdims=True) * (1.0 / DV)
                done = ((mixed - mu) * lax.rsqrt(sq - mu * mu + EPS_GROUP)).astype(BF16)
                rows = pl.ds(i * 256, 256)
                if s == 0:
                    for g in range(2):
                        at = pl.multiple_of((g * HEADS + c * 4 + h) * 128, 128)
                        ret[rows, pl.ds(at, 128)] = done[:, g * 128 : (g + 1) * 128]
                else:
                    ret_send[h, rows] = done
            if s == 1:
                for g in range(2):
                    at = pl.multiple_of((g * HEADS + c * 4 + h) * 128, 128)
                    pltpu.make_async_remote_copy(
                        ret_send.at[h, :, pl.ds(g * 128, 128)], ret.at[:, pl.ds(at, 128)],
                        rs.at[h], rr.at[h], device_id=mate, device_id_type=MESH,
                    ).start()
            return carry
        lax.fori_loop(0, 2, body, 0)

    def pass_out(piece):
        j = piece - O_FIRST
        pltpu.make_async_remote_copy(
            w.at[piece], w.at[piece + 4], os.at[j], orr.at[j], device_id=mate, device_id_type=MESH
        ).start()

    def out_copy(j, core):
        at = pl.multiple_of(core * 1024 + j * 256, 256)
        slot = j if core is c else j + 4
        return pltpu.make_async_copy(out_v.at[slot], out.at[0, :, pl.ds(at, 256)], out_sem.at[slot])

    def out_pieces(core):
        first = O_FIRST if core is c else O_FIRST + 4
        def body(j, carry):
            if core is not c:
                drain(w.at[0], orr.at[j])
            prod = jnp.dot(ret[...], w[first + j].reshape(D, 256), preferred_element_type=F32)
            out_v[first - O_FIRST + j] = prod.astype(BF16)
            out_copy(j, core).start()
            return carry
        lax.fori_loop(0, 4, body, 0)

    other = 1 - c

    tables()
    stage_p0(0)
    stage_p0(1)
    norm(0)
    stage_a(0)
    norm(1)
    norm_copy(0).start()
    stage_a(1)
    norm(2)
    norm_copy(1).start()
    stage_b(0)
    norm(3)
    norm_copy(2).start()
    stage_b(1)
    stage_p0(2)
    stage_p0(3)
    norm_copy(3).start()
    stage_c(0)
    rate_copy.wait()
    decays()
    stage_a(2)
    stage_a(3)
    stage_d(0)
    stage_c(1)
    stage_b(2)
    stage_b(3)
    for i in range(4):
        norm_copy(i).wait()
    stage_e(0)
    key_piece(0)
    value_piece(0)
    value_piece(1)
    local_states(0)
    stage_d(1)
    send_states(0)
    stage_c(2)
    stage_e(1)
    key_piece(1)
    value_piece(2)
    value_piece(3)
    local_states(1)
    scan_states(0)
    send_states(1)
    stage_d(2)
    send_prefixes(0)
    stage_c(3)
    stage_e(2)
    pass_out(O_FIRST)
    query_piece(0)
    scan_states(1)
    query_piece(1)
    send_prefixes(1)
    drain(p_recv.at[0, pl.ds(0, SHARDS - 1)], pr.at[0])
    retention(1, 0)
    stage_d(3)
    retention(0, 0)
    drain(p_recv.at[1, pl.ds(0, SHARDS - 1)], pr.at[1])
    retention(1, 1)
    retention(0, 1)
    stage_e(3)
    for piece in range(O_FIRST + 1, O_FIRST + 4):
        pass_out(piece)
    for h in range(4):
        drain(ret_send.at[0], rr.at[h])
    out_pieces(c)
    out_pieces(other)

    for wave in range(WAVES):
        finish_sends(wave)
    for half in range(2):
        drain(s_recv.at[half, pl.ds(0, SHARDS - 1)], ss.at[half])
        drain(p_recv.at[half, pl.ds(0, SHARDS - 1)], ps.at[half])
    for h in range(4):
        drain(ret_send.at[0], rs.at[h])
        drain(w.at[0], os.at[h])
    for j in range(4):
        out_copy(j, c).wait()
        out_copy(j, other).wait()


def body(tokens, norm_gain, w_query, w_key, w_value, w_out, decay_rate):
    high, low = rope_constants()
    any_spec = pl.BlockSpec(memory_space=pl.ANY)
    vmem = pl.BlockSpec(memory_space=pltpu.VMEM)
    dma = pltpu.SemaphoreType.DMA
    scratch = [
        pltpu.VMEM((16, 4, 4, 4, 32, 256), BF16),
        pltpu.VMEM((LEN, D), BF16),
        pltpu.VMEM((2, LEN, D), BF16),
        pltpu.VMEM((HEADS, 64), F32),
        pltpu.VMEM((LEN, DK), F32),
        pltpu.VMEM((LEN, DK), F32),
        pltpu.VMEM((2, 4, 4, 128), F32),
        pltpu.VMEM((2, 5, 4, 128), F32),
        pltpu.VMEM((2, 4, SHARDS, 128), F32),
        pltpu.VMEM((2, 4, LEN, DK), BF16),
        pltpu.VMEM((2, 4, LEN, DK), BF16),
        pltpu.VMEM((2, 4, LEN, DV), BF16),
        pltpu.VMEM((2, SHARDS, 32, DV), BF16),
        pltpu.VMEM((2, SHARDS, 32, DV), BF16),
        pltpu.VMEM((2, SHARDS, 32, DV), BF16),
        pltpu.VMEM((2, SHARDS, 32, DV), BF16),
        pltpu.VMEM((LEN, D), BF16),
        pltpu.VMEM((4, LEN, DV), BF16),
        pltpu.VMEM((8, LEN, 256), BF16),
        dma((4,)), dma((WAVES,)), dma((WAVES,)), dma((WAVES,)), dma, dma, dma((4,)), dma((4,)),
        dma((WAVES,)), dma((WAVES,)), dma((WAVES,)), dma((WAVES,)), dma((WAVES,)), dma((WAVES,)),
        dma((WAVES,)), dma((WAVES, 3, 2, 2)), dma((WAVES,)), dma((WAVES, 3, 2)),
        dma((2,)), dma((2,)), dma((2,)), dma((2,)), dma((4,)), dma((4,)), dma((4,)), dma((4,)), dma((8,)),
    ]
    return pl.pallas_call(
        kernel,
        out_shape=jax.ShapeDtypeStruct((1, LEN, D), BF16),
        in_specs=[any_spec, vmem, any_spec, any_spec, any_spec, any_spec, vmem, vmem, vmem],
        out_specs=any_spec,
        scratch_shapes=scratch,
        compiler_params=pltpu.CompilerParams(
            collective_id=0, has_side_effects=True, vmem_limit_bytes=60 * 1024 * 1024
        ),
    )(tokens, norm_gain[None], w_query, w_key, w_value, w_out, decay_rate[0], jnp.asarray(high), jnp.asarray(low))


def solution(mesh):
    split = Mesh(mesh.devices.reshape(4, 4, 4, 2), ("z", "y", "x", "c"))
    in_specs = (
        P(("x", "c"), ("z", "y"), None),
        P(),
        P(("z", "y", "x", "c"), None),
        P(("z", "y", "x", "c"), None),
        P(("z", "y", "x", "c"), None),
        P(("z", "y", "x", "c"), None),
        P(("x", "c"), None, None),
    )
    return jax.shard_map(
        body, mesh=split, in_specs=in_specs, out_specs=P(("x", "c"), ("z", "y"), None), check_vma=False
    )
```

time: 302 us -> 88.2 us (0.29)
  waiting for transfers between devices: 123 us -> 0 us
  Pallas kernels: 0 us -> 84.9 us
  local copies, waits for them, and re-layouts: 75.6 us -> 3.16 us
  matrix products: 46.9 us -> 0 us
  other arithmetic: 25.6 us -> 0 us
  blocking collectives: 15.5 us -> 0 us
  between operations: 14.2 us -> 0.01 us
    all_gather x5 -> x0, waiting for transfers between devices: 123 us -> none  [the longest x1 81.8 us: in_one_piece(): lax.all_gather(both, axis, axis=dim, tiled=True)]
    pallas_call x0 -> x1, Pallas kernels: none -> 84.9 us  [body(): pl.pallas_call(kernel, out_shape=jax.ShapeDtypeStruct((1, LEN, D), BF16),...]
    dot_general x7 -> x0, matrix products: 46.9 us -> none  [the longest x4 30.6 us: add_rows(): return jnp.dot(left, weight_piece, preferred_element_type=jnp.float32)]
    pad x4 -> x0, local copies, waits for them, and re-layouts: 24 us -> none  [retain(): lax.associative_scan(combine_pairs, (carried, local_state), axis=1)]
    another operation x6 -> x0, local copies, waits for them, and re-layouts: 14.3 us -> none  [the longest x4 8.32 us: rotate(): paired = stacked.reshape(stacked.shape[0], stacked.shape[1], -1, 2)]
    unnamed x31 -> x1, local copies, waits for them, and re-layouts: 16.6 us -> 3.16 us
    add x7 -> x0, other arithmetic: 8.53 us -> none  [the longest x3 4.94 us: combine_pairs(): later[0][..., None, None] * earlier[1] + later[1]]
    transpose x1 -> x0, local copies, waits for them, and re-layouts: 8.44 us -> none  [gather_in_order(): parts = parts.transpose(*back, *range(len(axes), parts.ndim))]
  transfers between devices with their start and end apart: 5 -> 0, of which waited for: 4 -> 0; matrix products, arithmetic and copies ran while one was open for 36% -> 0% of each run, Pallas kernels for 0% -> 0%
where the time goes in v1:
time: 88.2 us; the launch traced here: 88 us
  Pallas kernels  84.9 us (96%)
  local copies, waits for them, and re-layouts  3.16 us (4%)
    pallas_call x1, Pallas kernels, body(): pl.pallas_call(kernel, out_shape=jax.ShapeDtypeStruct((1, LEN, D), BF16),...  84.9 us
    unnamed x1, local copies, waits for them, and re-layouts  3.16 us

profile of v1, /device:TPU:1, one launch (start us, length us, event | category | flops | bytes accessed | tf_op | source)
XLA Modules:
  0.0 88.0 jit_solution(11360037867634340869)
XLA Ops:
  0.0 84.9 %shard_map.91 = bf16[1,512,2048]{2,1,0:T(8,128)(2,1)} custom-call(bf16[1,512,2048]{2,1,0:T(8,128)(2,1)} %tokens.1, f32[1,2048]{1,0:T(1,128)} %bitcast.2, bf16[16,1024]{1,0:T(8,128)(2,1)} %wq.1, bf16[16,1024]{1,0:T(8,128)(2,1)} %wk.1, bf16[16,2048]{1,0:T(8,128)(2,1)} %wv.1, bf16[16,2048]{1,0:T(8,128)(2,1)} %wo.1, f32[8,64]{1,0:T(8,128)} %bitcast.3, ...), custom_call_target="tpu_custom_call" | custom-call | tf_op jit(solution)/shard_map/pallas_call | solution.py:504
  84.9 3.2 %copy.11 = bf16[1,512,2048]{2,1,0:T(8,128)(2,1)} copy(bf16[1,512,2048]{2,1,0:T(8,128)(2,1)} %shard_map.91) | data formatting | bytes 4194304

commit v2 on v1

--- a/solution.py
+++ b/solution.py
@@ -29,7 +29,12 @@
 Q_PIECES = (6, 7)
 O_FIRST = 8
 WAVES = 4
-ORDERS = ((2, 1, 0), (1, 0, 2), (0, 2, 1))
+ORDERS = (
+    ((2, 1, 0), (1, 0, 2), (0, 2, 1)),
+    ((2, 1, 0), (1, 0, 2), (0, 2, 1)),
+    ((1, 2, 0), (0, 1, 2), (2, 0, 1)),
+    ((0, 2, 1), (1, 2, 0), (0, 1, 2)),
+)
 
 
 def rope_constants():
@@ -43,11 +48,11 @@
 
 
 def kernel(
-    tokens, gain, wq, wk, wv, wo, rates, high, low,
+    tokens, gain_in, wq, wk, wv, wo, rates_in, high_in, low_in,
     out,
-    w, x_raw, xn, rates2, cos_t, sin_t, rate_b, base_b, dec,
+    w, for_mate, x_raw, xn, gain, high, low, rates, rates2, cos_t, sin_t, rate_b, base_b, dec,
     keys, queries, values, s_send, s_recv, p_send, p_recv, ret, ret_send, out_v,
-    tok_sem, own_sem, mate_s, mate_r, rate_s, rate_r, xn_s, xn_r,
+    in_sem, tok_sem, own_sem, mate_s, mate_r, rate_s, rate_r, xn_s, xn_r,
     p1s, p1r, p2s, p2r, p2fs, p2fr, p3s, p3r, p3fs, p3fr,
     ss, sr, ps, pr, rs, rr, os, orr, out_sem,
 ):
@@ -56,10 +61,10 @@
     shard = z * 4 + y
     mate = (z, y, x, 1 - c)
 
-    def device(dim, step):
+    def device(dim, step, core=None):
         at = list(here)
         at[dim] = lax.rem(at[dim] + step, 4)
-        return (*at, c)
+        return (*at, c if core is None else core)
 
     def peer(step):
         to = lax.rem(shard + step, SHARDS)
@@ -90,37 +95,33 @@
         return todo
 
     own_rows = pl.ds(pl.multiple_of(c * 16, 16), 16)
+    other = 1 - c
+
+    barrier = pltpu.get_barrier_semaphore()
+    first_peers = [mate]
+    for dim in range(3):
+        for step in (1, 3, 2):
+            first_peers += [device(dim, step), device(dim, step, other)]
+    for dev in first_peers:
+        pl.semaphore_signal(barrier, inc=1, device_id=dev, device_id_type=MESH)
+
+    in_copies = [
+        pltpu.make_async_copy(gain_in, gain, in_sem.at[0]),
+        pltpu.make_async_copy(rates_in, rates, in_sem.at[1]),
+        pltpu.make_async_copy(high_in.at[:, pl.ds(pl.multiple_of(shard * 16, 16), 16)], high, in_sem.at[2]),
+        pltpu.make_async_copy(low_in, low, in_sem.at[3]),
+    ]
+    for cp in in_copies + tok_copies:
+        cp.start()
     for wave in range(WAVES):
         for src, piece, cols in pieces_of(wave, c):
             pltpu.make_async_copy(src, w.at[piece, z, y, x, own_rows, cols], own_sem.at[wave]).start()
-        if wave == 0:
-            for cp in tok_copies:
-                cp.start()
-
-    barrier = pltpu.get_barrier_semaphore()
-
-    def greet(step, carry):
-        _, dev = peer(step)
-        pl.semaphore_signal(barrier, inc=1, device_id=dev, device_id_type=MESH)
-        return carry
-
-    lax.fori_loop(1, SHARDS, greet, 0)
-    for step in range(1, 4):
-        pl.semaphore_signal(barrier, inc=1, device_id=device(2, step), device_id_type=MESH)
-    pl.semaphore_signal(barrier, inc=1, device_id=mate, device_id_type=MESH)
-    pl.semaphore_wait(barrier, 19)
-
-    for wave in range(WAVES):
-        for src, piece, cols in pieces_of(wave, 1 - c):
-            pltpu.make_async_remote_copy(
-                src, w.at[piece, z, y, x, own_rows, cols],
-                mate_s.at[wave], mate_r.at[wave], device_id=mate, device_id_type=MESH,
-            ).start()
-        if wave == 0:
-            rate_copy = pltpu.make_async_remote_copy(
-                rates, rates2, rate_s, rate_r, device_id=mate, device_id_type=MESH
-            )
-            rate_copy.start()
+        for src, piece, cols in pieces_of(wave, other):
+            pltpu.make_async_copy(src, for_mate.at[piece, :, cols], own_sem.at[wave]).start()
+    pl.semaphore_wait(barrier, len(first_peers))
+    rate_copy = pltpu.make_async_remote_copy(
+        rates_in, rates2, rate_s, rate_r, device_id=mate, device_id_type=MESH
+    )
 
     def part_slice(piece, where):
         idx = tuple(where.get(d, pl.ds(0, 4)) for d in range(3))
@@ -149,26 +150,32 @@
 
     HALF = (pl.ds(0, 2), pl.ds(2, 2))
 
-    def stage_p0(wave):
-        ref = w.at[three(wave), 0, 0, 0, pl.ds(0, 16)]
-        drain(ref, own_sem.at[wave])
-        drain(ref, mate_r.at[wave])
-        for part, (d1, d2, d3) in enumerate(ORDERS):
+    def stage_p(wave):
+        drain(w.at[three(wave), 0, 0, 0], own_sem.at[wave])
+        for part, (d1, d2, d3) in enumerate(ORDERS[wave]):
             piece = 3 * wave + part
-            own = part_slice(piece, {0: z, 1: y, 2: x})
+            own = w.at[piece, z, y, x, own_rows]
+            pltpu.make_async_remote_copy(
+                for_mate.at[piece], own, mate_s.at[wave], mate_r.at[wave], device_id=mate, device_id_type=MESH
+            ).start()
             for step in (1, 3, 2):
-                send(own, p1s.at[wave], p1r.at[wave], device(d1, step))
+                for src, core in ((own, c), (for_mate.at[piece], other)):
+                    pltpu.make_async_remote_copy(
+                        src, own, p1s.at[wave], p1r.at[wave],
+                        device_id=device(d1, step, core), device_id_type=MESH,
+                    ).start()
 
     def stage_a(wave):
+        drain(w.at[three(wave), 0, 0, 0, pl.ds(0, 16)], mate_r.at[wave])
         drain(p1_wait_ref(wave), p1r.at[wave])
-        for part, (d1, d2, d3) in enumerate(ORDERS):
+        for part, (d1, d2, d3) in enumerate(ORDERS[wave]):
             own = part_slice(3 * wave + part, {d2: here[d2], d3: here[d3]})
             for step in (1, 3):
                 send(own, p2s.at[wave], p2r.at[wave], device(d2, step))
 
     def stage_b(wave):
         drain(p2_wait_ref(wave), p2r.at[wave])
-        for part, (d1, d2, d3) in enumerate(ORDERS):
+        for part, (d1, d2, d3) in enumerate(ORDERS[wave]):
             for i, step in enumerate((1, 3)):
                 origin = lax.rem(here[d2] + 4 - step, 4)
                 src = part_slice(3 * wave + part, {d1: HALF[i], d2: origin, d3: here[d3]})
@@ -177,25 +184,46 @@
     def stage_c(wave):
         drain(p2f_wait_ref(wave), p2fr.at[wave])
         for sub in range(2):
-            for part, (d1, d2, d3) in enumerate(ORDERS):
+            for part, (d1, d2, d3) in enumerate(ORDERS[wave]):
                 for i, step in enumerate((1, 3)):
                     half = sub if i == 0 else 1 - sub
                     src = part_slice(3 * wave + part, {d2: HALF[half], d3: here[d3]})
                     send(src, p3s.at[wave], p3r.at[wave, part, i, sub], device(d3, step))
-
-    def stage_d(wave):
-        for part, (d1, d2, d3) in enumerate(ORDERS):
-            for i, step in enumerate((1, 3)):
-                drain(half_wait_ref(wave), p3r.at[wave, part, i, 0])
-                origin = lax.rem(here[d3] + 4 - step, 4)
-                src = part_slice(3 * wave + part, {d2: HALF[i], d3: origin})
-                send(src, p3fs.at[wave], p3fr.at[wave, part, i], device(d3, step))
-
-    def stage_e(wave):
         for part in range(3):
-            for i in range(2):
-                drain(half_wait_ref(wave), p3r.at[wave, part, i, 1])
-                drain(half_wait_ref(wave), p3fr.at[wave, part, i])
+            if 3 * wave + part >= O_FIRST:
+                d3 = ORDERS[wave][part][2]
+                pass_on(3 * wave + part, d3, here[d3])
+
+    def stage_d(wave, part):
+        d1, d2, d3 = ORDERS[wave][part]
+        for i, step in enumerate((1, 3)):
+            drain(half_wait_ref(wave), p3r.at[wave, part, i, 0])
+            origin = lax.rem(here[d3] + 4 - step, 4)
+            src = part_slice(3 * wave + part, {d2: HALF[i], d3: origin})
+            send(src, p3fs.at[wave, part], p3fr.at[wave, part, i], device(d3, step))
+
+    def pass_on(piece, d3, at):
+        j = piece - O_FIRST
+        pltpu.make_async_remote_copy(
+            part_slice(piece, {d3: at}), part_slice(piece + 4, {d3: at}),
+            os.at[j], orr.at[j], device_id=mate, device_id_type=MESH,
+        ).start()
+
+    def stage_e(wave, part):
+        piece = 3 * wave + part
+        d3 = ORDERS[wave][part][2]
+        for i, step in enumerate((1, 3)):
+            drain(half_wait_ref(wave), p3r.at[wave, part, i, 1])
+            if piece >= O_FIRST:
+                pass_on(piece, d3, lax.rem(here[d3] + 4 - step, 4))
+
+    def stage_f(wave, part):
+        piece = 3 * wave + part
+        d3 = ORDERS[wave][part][2]
+        for i in range(2):
+            drain(half_wait_ref(wave), p3fr.at[wave, part, i])
+        if piece >= O_FIRST:
+            pass_on(piece, d3, lax.rem(here[d3] + 2, 4))
 
     def finish_sends(wave):
         drain(w.at[three(wave), 0, 0, 0, pl.ds(0, 16)], mate_s.at[wave])
@@ -203,7 +231,8 @@
         drain(p2_wait_ref(wave), p2s.at[wave])
         drain(p2f_wait_ref(wave), p2fs.at[wave])
         drain(w.at[three(wave), pl.ds(0, 2)], p3s.at[wave])
-        drain(w.at[three(wave), 0], p3fs.at[wave])
+        for part in range(3):
+            drain(w.at[3 * wave, 0], p3fs.at[wave, part])
 
     def norm(i):
         rows = pl.ds(i * 128, 128)
@@ -223,8 +252,7 @@
         sign = jnp.where(lax.rem(lane, 2) == 0, -1.0, 1.0).astype(F32)
         cl, sl = low[0], low[1]
         for i in range(16):
-            at = shard * 16 + i
-            ch, sh = high[0, pl.ds(at, 1)], high[1, pl.ds(at, 1)]
+            ch, sh = high[0, pl.ds(i, 1)], high[1, pl.ds(i, 1)]
             cos_t[pl.ds(i * 32, 32)] = ch * cl - sh * sl
             sin_t[pl.ds(i * 32, 32)] = (sh * cl + ch * sl) * sign
 
@@ -367,96 +395,125 @@
             return carry
         lax.fori_loop(0, 2, body, 0)
 
-    def pass_out(piece):
-        j = piece - O_FIRST
-        pltpu.make_async_remote_copy(
-            w.at[piece], w.at[piece + 4], os.at[j], orr.at[j], device_id=mate, device_id_type=MESH
-        ).start()
-
     def out_copy(j, core):
         at = pl.multiple_of(core * 1024 + j * 256, 256)
         slot = j if core is c else j + 4
         return pltpu.make_async_copy(out_v.at[slot], out.at[0, :, pl.ds(at, 256)], out_sem.at[slot])
 
-    def out_pieces(core):
-        first = O_FIRST if core is c else O_FIRST + 4
-        def body(j, carry):
-            if core is not c:
-                drain(w.at[0], orr.at[j])
-            prod = jnp.dot(ret[...], w[first + j].reshape(D, 256), preferred_element_type=F32)
-            out_v[first - O_FIRST + j] = prod.astype(BF16)
-            out_copy(j, core).start()
-            return carry
-        lax.fori_loop(0, 4, body, 0)
-
-    other = 1 - c
-
+    def out_piece(core, j):
+        slot = j if core is c else j + 4
+        if core is not c:
+            drain(w.at[0], orr.at[j])
+        prod = jnp.dot(ret[...], w[O_FIRST + slot].reshape(D, 256), preferred_element_type=F32)
+        out_v[slot] = prod.astype(BF16)
+        out_copy(j, core).start()
+
+    def wait_prefixes(half):
+        drain(p_recv.at[half, pl.ds(0, SHARDS - 1)], pr.at[half])
+
+    def wait_retained():
+        for h in range(4):
+            drain(ret_send.at[0], rr.at[h])
+
+    stage_p(0)
+    stage_p(1)
+    stage_p(2)
+    stage_p(3)
+    stage_a(0)
+    stage_a(2)
+    for cp in in_copies:
+        cp.wait()
+    norm(0)
+    stage_a(1)
+    norm(1)
+    stage_b(0)
+    stage_b(2)
+    stage_b(1)
+    stage_c(0)
+    stage_d(0, 0)
+    stage_d(0, 1)
     tables()
-    stage_p0(0)
-    stage_p0(1)
-    norm(0)
-    stage_a(0)
-    norm(1)
     norm_copy(0).start()
-    stage_a(1)
+    stage_c(1)
+    norm_copy(1).start()
+    stage_e(0, 1)
+    rate_copy.start()
     norm(2)
-    norm_copy(1).start()
-    stage_b(0)
+    stage_a(3)
+    norm_copy(2).start()
     norm(3)
-    norm_copy(2).start()
-    stage_b(1)
-    stage_p0(2)
-    stage_p0(3)
     norm_copy(3).start()
-    stage_c(0)
+    stage_f(0, 1)
+    stage_d(0, 2)
+    stage_d(1, 1)
+    stage_e(0, 2)
+    stage_d(1, 0)
+    stage_d(1, 2)
     rate_copy.wait()
     decays()
-    stage_a(2)
-    stage_a(3)
-    stage_d(0)
-    stage_c(1)
-    stage_b(2)
-    stage_b(3)
+    stage_e(0, 0)
+    stage_f(0, 0)
+    stage_c(2)
     for i in range(4):
         norm_copy(i).wait()
-    stage_e(0)
+    value_piece(0)
     key_piece(0)
-    value_piece(0)
+    stage_f(0, 2)
+    stage_e(1, 2)
     value_piece(1)
     local_states(0)
-    stage_d(1)
+    stage_f(1, 2)
     send_states(0)
-    stage_c(2)
-    stage_e(1)
+    value_piece(3)
+    stage_e(1, 1)
+    stage_e(1, 0)
+    stage_d(2, 0)
+    stage_f(1, 1)
+    value_piece(2)
+    stage_f(1, 0)
     key_piece(1)
-    value_piece(2)
-    value_piece(3)
+    stage_b(3)
     local_states(1)
+    send_states(1)
+    stage_d(2, 1)
+    stage_c(3)
     scan_states(0)
-    send_states(1)
-    stage_d(2)
+    stage_e(2, 1)
     send_prefixes(0)
-    stage_c(3)
-    stage_e(2)
-    pass_out(O_FIRST)
+    stage_e(2, 0)
+    stage_f(2, 0)
+    scan_states(1)
+    send_prefixes(1)
+    stage_d(3, 2)
+    stage_e(3, 2)
+    stage_f(2, 1)
     query_piece(0)
-    scan_states(1)
     query_piece(1)
-    send_prefixes(1)
-    drain(p_recv.at[0, pl.ds(0, SHARDS - 1)], pr.at[0])
+    stage_d(2, 2)
+    wait_prefixes(0)
+    stage_d(3, 1)
+    retention(0, 0)
+    stage_e(2, 2)
+    stage_d(3, 0)
     retention(1, 0)
-    stage_d(3)
-    retention(0, 0)
-    drain(p_recv.at[1, pl.ds(0, SHARDS - 1)], pr.at[1])
+    stage_f(3, 2)
+    wait_prefixes(1)
     retention(1, 1)
     retention(0, 1)
-    stage_e(3)
-    for piece in range(O_FIRST + 1, O_FIRST + 4):
-        pass_out(piece)
-    for h in range(4):
-        drain(ret_send.at[0], rr.at[h])
-    out_pieces(c)
-    out_pieces(other)
+    stage_e(3, 1)
+    stage_f(2, 2)
+    stage_f(3, 1)
+    wait_retained()
+    stage_e(3, 0)
+    out_piece(c, 0)
+    out_piece(other, 3)
+    out_piece(c, 2)
+    out_piece(c, 3)
+    stage_f(3, 0)
+    out_piece(other, 2)
+    out_piece(other, 0)
+    out_piece(c, 1)
+    out_piece(other, 1)
 
     for wave in range(WAVES):
         finish_sends(wave)
@@ -474,12 +531,16 @@
 def body(tokens, norm_gain, w_query, w_key, w_value, w_out, decay_rate):
     high, low = rope_constants()
     any_spec = pl.BlockSpec(memory_space=pl.ANY)
-    vmem = pl.BlockSpec(memory_space=pltpu.VMEM)
     dma = pltpu.SemaphoreType.DMA
     scratch = [
         pltpu.VMEM((16, 4, 4, 4, 32, 256), BF16),
+        pltpu.VMEM((12, 16, 256), BF16),
         pltpu.VMEM((LEN, D), BF16),
         pltpu.VMEM((2, LEN, D), BF16),
+        pltpu.VMEM((1, D), F32),
+        pltpu.VMEM((2, 16, DK), F32),
+        pltpu.VMEM((2, 32, DK), F32),
+        pltpu.VMEM((HEADS, 64), F32),
         pltpu.VMEM((HEADS, 64), F32),
         pltpu.VMEM((LEN, DK), F32),
         pltpu.VMEM((LEN, DK), F32),
@@ -496,15 +557,15 @@
         pltpu.VMEM((LEN, D), BF16),
         pltpu.VMEM((4, LEN, DV), BF16),
         pltpu.VMEM((8, LEN, 256), BF16),
-        dma((4,)), dma((WAVES,)), dma((WAVES,)), dma((WAVES,)), dma, dma, dma((4,)), dma((4,)),
+        dma((4,)), dma((4,)), dma((WAVES,)), dma((WAVES,)), dma((WAVES,)), dma, dma, dma((4,)), dma((4,)),
         dma((WAVES,)), dma((WAVES,)), dma((WAVES,)), dma((WAVES,)), dma((WAVES,)), dma((WAVES,)),
-        dma((WAVES,)), dma((WAVES, 3, 2, 2)), dma((WAVES,)), dma((WAVES, 3, 2)),
+        dma((WAVES,)), dma((WAVES, 3, 2, 2)), dma((WAVES, 3)), dma((WAVES, 3, 2)),
         dma((2,)), dma((2,)), dma((2,)), dma((2,)), dma((4,)), dma((4,)), dma((4,)), dma((4,)), dma((8,)),
     ]
     return pl.pallas_call(
         kernel,
         out_shape=jax.ShapeDtypeStruct((1, LEN, D), BF16),
-        in_specs=[any_spec, vmem, any_spec, any_spec, any_spec, any_spec, vmem, vmem, vmem],
+        in_specs=[any_spec] * 9,
         out_specs=any_spec,
         scratch_shapes=scratch,
         compiler_params=pltpu.CompilerParams(

time: 88.2 us -> 81.7 us (0.926)
  Pallas kernels: 84.9 us -> 78.4 us
    pallas_call x1, Pallas kernels: 84.9 us -> 78.4 us  [body(): pl.pallas_call(kernel, out_shape=jax.ShapeDtypeStruct((1, LEN, D), BF16),...]
where the time goes in v2:
time: 81.7 us; the launch traced here: 81.6 us
  Pallas kernels  78.4 us (96%)
  local copies, waits for them, and re-layouts  3.16 us (4%)
    pallas_call x1, Pallas kernels, body(): pl.pallas_call(kernel, out_shape=jax.ShapeDtypeStruct((1, LEN, D), BF16),...  78.4 us
    unnamed x1, local copies, waits for them, and re-layouts  3.16 us

profile of v2, /device:TPU:1, one launch (start us, length us, event | category | flops | bytes accessed | tf_op | source)
XLA Modules:
  0.0 81.6 jit_solution(17827078935316329786)
XLA Ops:
  0.0 78.4 %shard_map.91 = bf16[1,512,2048]{2,1,0:T(8,128)(2,1)} custom-call(bf16[1,512,2048]{2,1,0:T(8,128)(2,1)} %tokens.1, f32[1,2048]{1,0:T(1,128)} %bitcast.2, bf16[16,1024]{1,0:T(8,128)(2,1)} %wq.1, bf16[16,1024]{1,0:T(8,128)(2,1)} %wk.1, bf16[16,2048]{1,0:T(8,128)(2,1)} %wv.1, bf16[16,2048]{1,0:T(8,128)(2,1)} %wo.1, f32[8,64]{1,0:T(8,128)} %bitcast.3, ...), custom_call_target="tpu_custom_call" | custom-call | tf_op jit(solution)/shard_map/pallas_call | solution.py:565
  78.4 3.2 %copy.11 = bf16[1,512,2048]{2,1,0:T(8,128)(2,1)} copy(bf16[1,512,2048]{2,1,0:T(8,128)(2,1)} %shard_map.91) | data formatting | bytes 4194304

commit v3 on v2

--- a/solution.py
+++ b/solution.py
@@ -51,10 +51,10 @@
     tokens, gain_in, wq, wk, wv, wo, rates_in, high_in, low_in,
     out,
     w, for_mate, x_raw, xn, gain, high, low, rates, rates2, cos_t, sin_t, rate_b, base_b, dec,
-    keys, queries, values, s_send, s_recv, p_send, p_recv, ret, ret_send, out_v,
+    keys, queries, values, s_send, s_recv, p_send, p_recv, ret, ret_send,
     in_sem, tok_sem, own_sem, mate_s, mate_r, rate_s, rate_r, xn_s, xn_r,
     p1s, p1r, p2s, p2r, p2fs, p2fr, p3s, p3r, p3fs, p3fr,
-    ss, sr, ps, pr, rs, rr, os, orr, out_sem,
+    ss, sr, ps, pr, rs, rr, os, orr,
 ):
     z, y, x, c = (lax.axis_index(a) for a in ("z", "y", "x", "c"))
     here = (z, y, x)
@@ -286,44 +286,39 @@
             parts.append(rot[n * BLOCK : (n + 1) * BLOCK] * (jnp.exp(e * sign) * scale))
         return jnp.concatenate(parts, axis=0).astype(BF16)
 
-    def project(s, piece):
-        return jnp.dot(xn[s], w[piece].reshape(D, 256), preferred_element_type=F32)
+    def project(piece):
+        return jnp.dot(
+            xn[...].reshape(2 * LEN, D), w[piece].reshape(D, 256), preferred_element_type=F32
+        ).reshape(2, LEN, 256)
 
     def key_piece(j):
-        def body(s, carry):
-            prod = project(s, K_PIECES[j])
+        prod = project(K_PIECES[j])
+        for s in range(2):
             for hh in range(2):
                 h = 2 * j + hh
-                keys[s, h] = turned(prod[:, hh * 128 : (hh + 1) * 128], s, h, 1.0, DK ** (-0.5))
-            return carry
-        lax.fori_loop(0, 2, body, 0)
+                keys[s, h] = turned(prod[s, :, hh * 128 : (hh + 1) * 128], s, h, 1.0, DK ** (-0.5))
 
     def query_piece(j):
-        def body(s, carry):
-            prod = project(s, Q_PIECES[j])
+        prod = project(Q_PIECES[j])
+        for s in range(2):
             for hh in range(2):
                 h = 2 * j + hh
-                queries[s, h] = turned(prod[:, hh * 128 : (hh + 1) * 128], s, h, -1.0, 1.0)
-            return carry
-        lax.fori_loop(0, 2, body, 0)
+                queries[s, h] = turned(prod[s, :, hh * 128 : (hh + 1) * 128], s, h, -1.0, 1.0)
 
     def value_piece(h):
-        def body(s, carry):
-            values[s, h] = project(s, V_PIECES[h]).astype(BF16)
-            return carry
-        lax.fori_loop(0, 2, body, 0)
+        prod = project(V_PIECES[h])
+        for s in range(2):
+            values[s, h] = prod[s].astype(BF16)
 
     def local_states(half):
-        def body(p, carry):
-            s, h = lax.div(p, 2), half * 2 + lax.rem(p, 2)
+        for p in range(4):
+            s, h = p // 2, half * 2 + p % 2
             st = lax.dot_general(
                 keys[s, h], values[s, h], (((0,), (0,)), ((), ())), preferred_element_type=F32
             )
             e = jnp.exp(-base_b[s, 4, pl.ds(h, 1)])
             e = jnp.concatenate([e, e], axis=1)
             s_send[half, pl.ds(p * 4, 4)] = (st * e).astype(BF16).reshape(4, 32, DV)
-            return carry
-        lax.fori_loop(0, 4, body, 0)
         s_recv[half, shard] = s_send[half, shard]
 
     def send_states(half):
@@ -360,7 +355,7 @@
     def retention(s, half):
         row = lax.broadcasted_iota(jnp.int32, (256, 256), 0)
         col = lax.broadcasted_iota(jnp.int32, (256, 256), 1)
-        def body(hh, carry):
+        for hh in range(2):
             h = half * 2 + hh
             p = s * 2 + hh
             before = p_recv[half, pl.ds(p * 4, 4)].reshape(DK, DV)
@@ -392,21 +387,14 @@
                         ret_send.at[h, :, pl.ds(g * 128, 128)], ret.at[:, pl.ds(at, 128)],
                         rs.at[h], rr.at[h], device_id=mate, device_id_type=MESH,
                     ).start()
-            return carry
-        lax.fori_loop(0, 2, body, 0)
-
-    def out_copy(j, core):
-        at = pl.multiple_of(core * 1024 + j * 256, 256)
-        slot = j if core is c else j + 4
-        return pltpu.make_async_copy(out_v.at[slot], out.at[0, :, pl.ds(at, 256)], out_sem.at[slot])
 
     def out_piece(core, j):
         slot = j if core is c else j + 4
         if core is not c:
             drain(w.at[0], orr.at[j])
         prod = jnp.dot(ret[...], w[O_FIRST + slot].reshape(D, 256), preferred_element_type=F32)
-        out_v[slot] = prod.astype(BF16)
-        out_copy(j, core).start()
+        at = pl.multiple_of(core * 1024 + j * 256, 256)
+        out[0, :, pl.ds(at, 256)] = prod.astype(BF16)
 
     def wait_prefixes(half):
         drain(p_recv.at[half, pl.ds(0, SHARDS - 1)], pr.at[half])
@@ -414,6 +402,9 @@
     def wait_retained():
         for h in range(4):
             drain(ret_send.at[0], rr.at[h])
+
+    def block(step, *args):
+        pl.when(z < 4)(functools.partial(step, *args))
 
     stage_p(0)
     stage_p(1)
@@ -423,25 +414,25 @@
     stage_a(2)
     for cp in in_copies:
         cp.wait()
-    norm(0)
+    block(norm, 0)
     stage_a(1)
-    norm(1)
+    block(norm, 1)
     stage_b(0)
     stage_b(2)
     stage_b(1)
     stage_c(0)
     stage_d(0, 0)
     stage_d(0, 1)
-    tables()
+    block(tables)
     norm_copy(0).start()
     stage_c(1)
     norm_copy(1).start()
     stage_e(0, 1)
     rate_copy.start()
-    norm(2)
+    block(norm, 2)
     stage_a(3)
     norm_copy(2).start()
-    norm(3)
+    block(norm, 3)
     norm_copy(3).start()
     stage_f(0, 1)
     stage_d(0, 2)
@@ -450,70 +441,70 @@
     stage_d(1, 0)
     stage_d(1, 2)
     rate_copy.wait()
-    decays()
+    block(decays)
     stage_e(0, 0)
     stage_f(0, 0)
     stage_c(2)
     for i in range(4):
         norm_copy(i).wait()
-    value_piece(0)
-    key_piece(0)
+    block(value_piece, 0)
+    block(key_piece, 0)
     stage_f(0, 2)
     stage_e(1, 2)
-    value_piece(1)
-    local_states(0)
+    block(value_piece, 1)
+    block(local_states, 0)
     stage_f(1, 2)
     send_states(0)
-    value_piece(3)
+    block(value_piece, 3)
     stage_e(1, 1)
     stage_e(1, 0)
     stage_d(2, 0)
     stage_f(1, 1)
-    value_piece(2)
+    block(value_piece, 2)
     stage_f(1, 0)
-    key_piece(1)
+    block(key_piece, 1)
     stage_b(3)
-    local_states(1)
+    block(local_states, 1)
     send_states(1)
     stage_d(2, 1)
     stage_c(3)
-    scan_states(0)
+    block(scan_states, 0)
     stage_e(2, 1)
     send_prefixes(0)
     stage_e(2, 0)
     stage_f(2, 0)
-    scan_states(1)
+    block(scan_states, 1)
     send_prefixes(1)
     stage_d(3, 2)
     stage_e(3, 2)
     stage_f(2, 1)
-    query_piece(0)
-    query_piece(1)
+    block(query_piece, 0)
+    block(query_piece, 1)
     stage_d(2, 2)
     wait_prefixes(0)
     stage_d(3, 1)
-    retention(0, 0)
+    block(retention, 0, 0)
     stage_e(2, 2)
     stage_d(3, 0)
-    retention(1, 0)
+    block(retention, 1, 0)
     stage_f(3, 2)
     wait_prefixes(1)
-    retention(1, 1)
-    retention(0, 1)
+    block(retention, 1, 1)
+    block(retention, 0, 1)
     stage_e(3, 1)
     stage_f(2, 2)
     stage_f(3, 1)
     wait_retained()
     stage_e(3, 0)
-    out_piece(c, 0)
-    out_piece(other, 3)
-    out_piece(c, 2)
-    out_piece(c, 3)
+    block(out_piece, c, 0)
+    block(out_piece, other, 3)
+    block(out_piece, c, 2)
+    block(out_piece, c, 3)
     stage_f(3, 0)
-    out_piece(other, 2)
-    out_piece(other, 0)
-    out_piece(c, 1)
-    out_piece(other, 1)
+    block(out_piece, other, 2)
+    block(out_piece, other, 0)
+    block(out_piece, c, 1)
+    block(out_piece, other, 1)
 
     for wave in range(WAVES):
         finish_sends(wave)
@@ -523,9 +514,6 @@
     for h in range(4):
         drain(ret_send.at[0], rs.at[h])
         drain(w.at[0], os.at[h])
-    for j in range(4):
-        out_copy(j, c).wait()
-        out_copy(j, other).wait()
 
 
 def body(tokens, norm_gain, w_query, w_key, w_value, w_out, decay_rate):
@@ -556,22 +544,25 @@
         pltpu.VMEM((2, SHARDS, 32, DV), BF16),
         pltpu.VMEM((LEN, D), BF16),
         pltpu.VMEM((4, LEN, DV), BF16),
-        pltpu.VMEM((8, LEN, 256), BF16),
         dma((4,)), dma((4,)), dma((WAVES,)), dma((WAVES,)), dma((WAVES,)), dma, dma, dma((4,)), dma((4,)),
         dma((WAVES,)), dma((WAVES,)), dma((WAVES,)), dma((WAVES,)), dma((WAVES,)), dma((WAVES,)),
         dma((WAVES,)), dma((WAVES, 3, 2, 2)), dma((WAVES, 3)), dma((WAVES, 3, 2)),
-        dma((2,)), dma((2,)), dma((2,)), dma((2,)), dma((4,)), dma((4,)), dma((4,)), dma((4,)), dma((8,)),
+        dma((2,)), dma((2,)), dma((2,)), dma((2,)), dma((4,)), dma((4,)), dma((4,)), dma((4,)),
     ]
+    args = (
+        tokens, norm_gain[None], w_query, w_key, w_value, w_out, decay_rate[0],
+        jnp.asarray(high), jnp.asarray(low),
+    )
     return pl.pallas_call(
         kernel,
         out_shape=jax.ShapeDtypeStruct((1, LEN, D), BF16),
         in_specs=[any_spec] * 9,
-        out_specs=any_spec,
+        out_specs=pl.BlockSpec(memory_space=pltpu.VMEM),
         scratch_shapes=scratch,
         compiler_params=pltpu.CompilerParams(
-            collective_id=0, has_side_effects=True, vmem_limit_bytes=60 * 1024 * 1024
+            collective_id=0, has_side_effects=True, vmem_limit_bytes=44 * 1024 * 1024
         ),
-    )(tokens, norm_gain[None], w_query, w_key, w_value, w_out, decay_rate[0], jnp.asarray(high), jnp.asarray(low))
+    )(*(pltpu.with_memory_space_constraint(a, pltpu.HBM) for a in args))
 
 
 def solution(mesh):

time: 81.7 us -> 78.4 us (0.960)
  local copies, waits for them, and re-layouts: 3.16 us -> 1.32 us
  Pallas kernels: 78.4 us -> 77 us
    unnamed x1, local copies, waits for them, and re-layouts: 3.16 us -> 1.32 us
    pallas_call x1, Pallas kernels: 78.4 us -> 77 us  [body(): pl.pallas_call(kernel, out_shape=jax.ShapeDtypeStruct((1, LEN, D), BF16),...]
where the time goes in v3:
time: 78.4 us; the launch traced here: 78.3 us
  Pallas kernels  77 us (98%)
  local copies, waits for them, and re-layouts  1.32 us (2%)
    pallas_call x1, Pallas kernels, body(): pl.pallas_call(kernel, out_shape=jax.ShapeDtypeStruct((1, LEN, D), BF16),...  77 us

profile of v3, /device:TPU:1, one launch (start us, length us, event | category | flops | bytes accessed | tf_op | source)
XLA Modules:
  0.0 78.3 jit_solution(5962120451020051779)
XLA Ops:
  0.0 77.0 %shard_map.91 = bf16[1,512,2048]{2,1,0:T(8,128)(2,1)S(1)} custom-call(bf16[1,512,2048]{2,1,0:T(8,128)(2,1)} %tokens.1, f32[1,2048]{1,0:T(1,128)} %bitcast.2, bf16[16,1024]{1,0:T(8,128)(2,1)} %wq.1, bf16[16,1024]{1,0:T(8,128)(2,1)} %wk.1, bf16[16,2048]{1,0:T(8,128)(2,1)} %wv.1, bf16[16,2048]{1,0:T(8,128)(2,1)} %wo.1, f32[8,64]{1,0:T(8,128)} %bitcast.3, ...), custom_call_target="tpu_custom_call" | custom-call | tf_op jit(solution)/shard_map/pallas_call | solution.py:556
  77.0 1.3 %copy.11 = bf16[1,512,2048]{2,1,0:T(8,128)(2,1)} copy(bf16[1,512,2048]{2,1,0:T(8,128)(2,1)S(1)} %shard_map.91) | data formatting | bytes 4194304

commit v4 on v3

--- a/solution.py
+++ b/solution.py
@@ -24,17 +24,32 @@
 EPS_GROUP = 0.01
 ROPE_BASE = 10000.0
 
-K_PIECES = (0, 3)
-V_PIECES = (1, 2, 4, 5)
-Q_PIECES = (6, 7)
-O_FIRST = 8
-WAVES = 4
-ORDERS = (
-    ((2, 1, 0), (1, 0, 2), (0, 2, 1)),
-    ((2, 1, 0), (1, 0, 2), (0, 2, 1)),
-    ((1, 2, 0), (0, 1, 2), (2, 0, 1)),
-    ((0, 2, 1), (1, 2, 0), (0, 1, 2)),
+PLAN = (
+    (((1, 2, 0), "Q"), ((0, 1, 2), "K"), ((2, 0, 1), "V")),
+    (((2, 1, 0), "KV"), ((1, 0, 2), "VVV"), ((0, 2, 1), "KKV")),
+    (((2, 1, 0), "VV"), ((0, 2, 1), "Q"), ((1, 0, 2), "QQOO")),
+    (((2, 0, 1), "OO"), ((2, 1, 0), "O"), ((2, 1, 0), "O")),
+    (((0, 1, 2), "OO"), ((0, 2, 1), ""), ((2, 0, 1), "")),
 )
+WAVES = len(PLAN)
+PIECES = 24
+KINDS = "".join(kinds for wave in PLAN for _, kinds in wave)
+
+
+def ranges():
+    at, parts, whole = 0, [], []
+    for wave in PLAN:
+        first, mine = at, []
+        for order, kinds in wave:
+            mine.append((order, at, len(kinds)))
+            at += len(kinds)
+        parts.append(mine)
+        whole.append((first, at - first))
+    return parts, whole
+
+
+PARTS, WHOLE = ranges()
+AT = {kind: [i for i, k in enumerate(KINDS) if k == kind] for kind in "KVQO"}
 
 
 def rope_constants():
@@ -76,23 +91,16 @@
         cp = pltpu.make_async_copy(tokens.at[0, rows], x_raw.at[rows], tok_sem.at[i])
         tok_copies.append(cp)
 
-    def pieces_of(wave, core):
-        todo = []
-        for piece in range(3 * wave, 3 * wave + 3):
-            if piece in K_PIECES or piece in Q_PIECES:
-                ref = wk if piece in K_PIECES else wq
-                j = K_PIECES.index(piece) if piece in K_PIECES else Q_PIECES.index(piece)
-                at = pl.multiple_of(core * 512 + j * 256, 256)
-                todo.append((ref.at[:, pl.ds(at, 256)], piece, pl.ds(0, 256)))
-            elif piece in V_PIECES:
-                h = V_PIECES.index(piece)
-                for s in range(2):
-                    at = pl.multiple_of(core * 512 + (s * 1024 + h * 128), 128)
-                    todo.append((wv.at[:, pl.ds(at, 128)], piece, pl.ds(s * 128, 128)))
-            else:
-                at = pl.multiple_of(core * 1024 + (piece - O_FIRST) * 256, 256)
-                todo.append((wo.at[:, pl.ds(at, 256)], piece, pl.ds(0, 256)))
-        return todo
+    def columns_of(piece, core):
+        kind = KINDS[piece]
+        i = AT[kind].index(piece)
+        if kind == "V":
+            ref, at = wv, core * 512 + (i % 2 * 1024 + i // 2 * 128)
+        elif kind == "O":
+            ref, at = wo, core * 1024 + i * 128
+        else:
+            ref, at = wk if kind == "K" else wq, core * 512 + i * 128
+        return ref.at[:, pl.ds(pl.multiple_of(at, 128), 128)]
 
     own_rows = pl.ds(pl.multiple_of(c * 16, 16), 16)
     other = 1 - c
@@ -113,19 +121,17 @@
     ]
     for cp in in_copies + tok_copies:
         cp.start()
-    for wave in range(WAVES):
-        for src, piece, cols in pieces_of(wave, c):
-            pltpu.make_async_copy(src, w.at[piece, z, y, x, own_rows, cols], own_sem.at[wave]).start()
-        for src, piece, cols in pieces_of(wave, other):
-            pltpu.make_async_copy(src, for_mate.at[piece, :, cols], own_sem.at[wave]).start()
+    for wave, (first, count) in enumerate(WHOLE):
+        for piece in range(first, first + count):
+            pltpu.make_async_copy(columns_of(piece, c), w.at[piece, z, y, x, own_rows], own_sem.at[wave]).start()
+            pltpu.make_async_copy(columns_of(piece, other), for_mate.at[piece], own_sem.at[wave]).start()
     pl.semaphore_wait(barrier, len(first_peers))
     rate_copy = pltpu.make_async_remote_copy(
         rates_in, rates2, rate_s, rate_r, device_id=mate, device_id_type=MESH
     )
 
-    def part_slice(piece, where):
-        idx = tuple(where.get(d, pl.ds(0, 4)) for d in range(3))
-        return w.at[(piece, *idx)]
+    def part_slice(first, count, where):
+        return w.at[(pl.ds(first, count), *(where.get(d, pl.ds(0, 4)) for d in range(3)))]
 
     def send(src, ssem, rsem, dev):
         pltpu.make_async_remote_copy(src, src, ssem, rsem, device_id=dev, device_id_type=MESH).start()
@@ -133,106 +139,109 @@
     def drain(ref, sem):
         pltpu.make_async_copy(ref, ref, sem).wait()
 
-    def three(wave):
-        return pl.ds(3 * wave, 3)
+    def rows_of(wave):
+        return pl.ds(*WHOLE[wave])
 
     def p1_wait_ref(wave):
-        return w.at[three(wave), 0, 0, pl.ds(0, 3)]
+        return w.at[rows_of(wave), 0, 0, pl.ds(0, 3)]
 
     def p2_wait_ref(wave):
-        return w.at[three(wave), pl.ds(0, 2), 0]
+        return w.at[rows_of(wave), pl.ds(0, 2), 0]
 
     def p2f_wait_ref(wave):
-        return w.at[three(wave), 0, 0]
-
-    def half_wait_ref(wave):
-        return w.at[3 * wave, pl.ds(0, 2), 0]
+        return w.at[rows_of(wave), 0, 0]
+
+    def mate_wait_ref(wave):
+        return w.at[rows_of(wave), 0, 0, 0, pl.ds(0, 16)]
+
+    def half_wait_ref(count):
+        return w.at[pl.ds(0, count), pl.ds(0, 2), 0]
 
     HALF = (pl.ds(0, 2), pl.ds(2, 2))
 
+    def parts_of(wave):
+        return [(part, *it) for part, it in enumerate(PARTS[wave]) if it[2]]
+
     def stage_p(wave):
-        drain(w.at[three(wave), 0, 0, 0], own_sem.at[wave])
-        for part, (d1, d2, d3) in enumerate(ORDERS[wave]):
-            piece = 3 * wave + part
-            own = w.at[piece, z, y, x, own_rows]
+        drain(w.at[rows_of(wave), 0, 0, 0], own_sem.at[wave])
+        for part, (d1, d2, d3), first, count in parts_of(wave):
+            pieces = pl.ds(first, count)
+            own = w.at[pieces, z, y, x, own_rows]
+            theirs = for_mate.at[pieces]
             pltpu.make_async_remote_copy(
-                for_mate.at[piece], own, mate_s.at[wave], mate_r.at[wave], device_id=mate, device_id_type=MESH
+                theirs, own, mate_s.at[wave], mate_r.at[wave], device_id=mate, device_id_type=MESH
             ).start()
             for step in (1, 3, 2):
-                for src, core in ((own, c), (for_mate.at[piece], other)):
+                for src, core in ((own, c), (theirs, other)):
                     pltpu.make_async_remote_copy(
                         src, own, p1s.at[wave], p1r.at[wave],
                         device_id=device(d1, step, core), device_id_type=MESH,
                     ).start()
 
     def stage_a(wave):
-        drain(w.at[three(wave), 0, 0, 0, pl.ds(0, 16)], mate_r.at[wave])
+        drain(mate_wait_ref(wave), mate_r.at[wave])
         drain(p1_wait_ref(wave), p1r.at[wave])
-        for part, (d1, d2, d3) in enumerate(ORDERS[wave]):
-            own = part_slice(3 * wave + part, {d2: here[d2], d3: here[d3]})
+        for part, (d1, d2, d3), first, count in parts_of(wave):
+            own = part_slice(first, count, {d2: here[d2], d3: here[d3]})
             for step in (1, 3):
                 send(own, p2s.at[wave], p2r.at[wave], device(d2, step))
 
     def stage_b(wave):
         drain(p2_wait_ref(wave), p2r.at[wave])
-        for part, (d1, d2, d3) in enumerate(ORDERS[wave]):
+        for part, (d1, d2, d3), first, count in parts_of(wave):
             for i, step in enumerate((1, 3)):
                 origin = lax.rem(here[d2] + 4 - step, 4)
-                src = part_slice(3 * wave + part, {d1: HALF[i], d2: origin, d3: here[d3]})
+                src = part_slice(first, count, {d1: HALF[i], d2: origin, d3: here[d3]})
                 send(src, p2fs.at[wave], p2fr.at[wave], device(d2, step))
 
     def stage_c(wave):
         drain(p2f_wait_ref(wave), p2fr.at[wave])
         for sub in range(2):
-            for part, (d1, d2, d3) in enumerate(ORDERS[wave]):
+            for part, (d1, d2, d3), first, count in parts_of(wave):
                 for i, step in enumerate((1, 3)):
                     half = sub if i == 0 else 1 - sub
-                    src = part_slice(3 * wave + part, {d2: HALF[half], d3: here[d3]})
+                    src = part_slice(first, count, {d2: HALF[half], d3: here[d3]})
                     send(src, p3s.at[wave], p3r.at[wave, part, i, sub], device(d3, step))
-        for part in range(3):
-            if 3 * wave + part >= O_FIRST:
-                d3 = ORDERS[wave][part][2]
-                pass_on(3 * wave + part, d3, here[d3])
+        for part, (d1, d2, d3), first, count in parts_of(wave):
+            pass_on(first, count, d3, here[d3])
 
     def stage_d(wave, part):
-        d1, d2, d3 = ORDERS[wave][part]
+        (d1, d2, d3), first, count = PARTS[wave][part]
         for i, step in enumerate((1, 3)):
-            drain(half_wait_ref(wave), p3r.at[wave, part, i, 0])
+            drain(half_wait_ref(count), p3r.at[wave, part, i, 0])
             origin = lax.rem(here[d3] + 4 - step, 4)
-            src = part_slice(3 * wave + part, {d2: HALF[i], d3: origin})
+            src = part_slice(first, count, {d2: HALF[i], d3: origin})
             send(src, p3fs.at[wave, part], p3fr.at[wave, part, i], device(d3, step))
 
-    def pass_on(piece, d3, at):
-        j = piece - O_FIRST
-        pltpu.make_async_remote_copy(
-            part_slice(piece, {d3: at}), part_slice(piece + 4, {d3: at}),
-            os.at[j], orr.at[j], device_id=mate, device_id_type=MESH,
-        ).start()
+    def pass_on(first, count, d3, at):
+        for piece in range(first, first + count):
+            if KINDS[piece] == "O":
+                j = AT["O"].index(piece)
+                pltpu.make_async_remote_copy(
+                    part_slice(piece, 1, {d3: at}), part_slice(PIECES + j, 1, {d3: at}),
+                    os.at[j], orr.at[j], device_id=mate, device_id_type=MESH,
+                ).start()
 
     def stage_e(wave, part):
-        piece = 3 * wave + part
-        d3 = ORDERS[wave][part][2]
+        (d1, d2, d3), first, count = PARTS[wave][part]
         for i, step in enumerate((1, 3)):
-            drain(half_wait_ref(wave), p3r.at[wave, part, i, 1])
-            if piece >= O_FIRST:
-                pass_on(piece, d3, lax.rem(here[d3] + 4 - step, 4))
+            drain(half_wait_ref(count), p3r.at[wave, part, i, 1])
+            pass_on(first, count, d3, lax.rem(here[d3] + 4 - step, 4))
 
     def stage_f(wave, part):
-        piece = 3 * wave + part
-        d3 = ORDERS[wave][part][2]
+        (d1, d2, d3), first, count = PARTS[wave][part]
         for i in range(2):
-            drain(half_wait_ref(wave), p3fr.at[wave, part, i])
-        if piece >= O_FIRST:
-            pass_on(piece, d3, lax.rem(here[d3] + 2, 4))
+            drain(half_wait_ref(count), p3fr.at[wave, part, i])
+        pass_on(first, count, d3, lax.rem(here[d3] + 2, 4))
 
     def finish_sends(wave):
-        drain(w.at[three(wave), 0, 0, 0, pl.ds(0, 16)], mate_s.at[wave])
+        drain(mate_wait_ref(wave), mate_s.at[wave])
         drain(p1_wait_ref(wave), p1s.at[wave])
         drain(p2_wait_ref(wave), p2s.at[wave])
         drain(p2f_wait_ref(wave), p2fs.at[wave])
-        drain(w.at[three(wave), pl.ds(0, 2)], p3s.at[wave])
-        for part in range(3):
-            drain(w.at[3 * wave, 0], p3fs.at[wave, part])
+        drain(w.at[rows_of(wave), pl.ds(0, 2)], p3s.at[wave])
+        for part, order, first, count in parts_of(wave):
+            drain(w.at[pl.ds(first, count), 0], p3fs.at[wave, part])
 
     def norm(i):
         rows = pl.ds(i * 128, 128)
@@ -286,27 +295,30 @@
             parts.append(rot[n * BLOCK : (n + 1) * BLOCK] * (jnp.exp(e * sign) * scale))
         return jnp.concatenate(parts, axis=0).astype(BF16)
 
-    def project(piece):
+    def pair(pieces):
+        return jnp.concatenate([w[piece].reshape(D, 128) for piece in pieces], axis=1)
+
+    def project(kind, j):
         return jnp.dot(
-            xn[...].reshape(2 * LEN, D), w[piece].reshape(D, 256), preferred_element_type=F32
+            xn[...].reshape(2 * LEN, D), pair(AT[kind][2 * j : 2 * j + 2]), preferred_element_type=F32
         ).reshape(2, LEN, 256)
 
     def key_piece(j):
-        prod = project(K_PIECES[j])
+        prod = project("K", j)
         for s in range(2):
             for hh in range(2):
                 h = 2 * j + hh
                 keys[s, h] = turned(prod[s, :, hh * 128 : (hh + 1) * 128], s, h, 1.0, DK ** (-0.5))
 
     def query_piece(j):
-        prod = project(Q_PIECES[j])
+        prod = project("Q", j)
         for s in range(2):
             for hh in range(2):
                 h = 2 * j + hh
                 queries[s, h] = turned(prod[s, :, hh * 128 : (hh + 1) * 128], s, h, -1.0, 1.0)
 
     def value_piece(h):
-        prod = project(V_PIECES[h])
+        prod = project("V", h)
         for s in range(2):
             values[s, h] = prod[s].astype(BF16)
 
@@ -389,10 +401,14 @@
                     ).start()
 
     def out_piece(core, j):
-        slot = j if core is c else j + 4
-        if core is not c:
-            drain(w.at[0], orr.at[j])
-        prod = jnp.dot(ret[...], w[O_FIRST + slot].reshape(D, 256), preferred_element_type=F32)
+        pieces = (2 * j, 2 * j + 1)
+        if core is c:
+            pieces = [AT["O"][i] for i in pieces]
+        else:
+            for i in pieces:
+                drain(w.at[0], orr.at[i])
+            pieces = [PIECES + i for i in pieces]
+        prod = jnp.dot(ret[...], pair(pieces), preferred_element_type=F32)
         at = pl.multiple_of(core * 1024 + j * 256, 256)
         out[0, :, pl.ds(at, 256)] = prod.astype(BF16)
 
@@ -403,108 +419,139 @@
         for h in range(4):
             drain(ret_send.at[0], rr.at[h])
 
-    def block(step, *args):
-        pl.when(z < 4)(functools.partial(step, *args))
-
-    stage_p(0)
-    stage_p(1)
-    stage_p(2)
-    stage_p(3)
-    stage_a(0)
-    stage_a(2)
-    for cp in in_copies:
-        cp.wait()
-    block(norm, 0)
-    stage_a(1)
-    block(norm, 1)
-    stage_b(0)
-    stage_b(2)
-    stage_b(1)
-    stage_c(0)
-    stage_d(0, 0)
-    stage_d(0, 1)
-    block(tables)
-    norm_copy(0).start()
-    stage_c(1)
-    norm_copy(1).start()
-    stage_e(0, 1)
-    rate_copy.start()
-    block(norm, 2)
-    stage_a(3)
-    norm_copy(2).start()
-    block(norm, 3)
-    norm_copy(3).start()
-    stage_f(0, 1)
-    stage_d(0, 2)
-    stage_d(1, 1)
-    stage_e(0, 2)
-    stage_d(1, 0)
-    stage_d(1, 2)
-    rate_copy.wait()
-    block(decays)
-    stage_e(0, 0)
-    stage_f(0, 0)
-    stage_c(2)
-    for i in range(4):
-        norm_copy(i).wait()
-    block(value_piece, 0)
-    block(key_piece, 0)
-    stage_f(0, 2)
-    stage_e(1, 2)
-    block(value_piece, 1)
-    block(local_states, 0)
-    stage_f(1, 2)
-    send_states(0)
-    block(value_piece, 3)
-    stage_e(1, 1)
-    stage_e(1, 0)
-    stage_d(2, 0)
-    stage_f(1, 1)
-    block(value_piece, 2)
-    stage_f(1, 0)
-    block(key_piece, 1)
-    stage_b(3)
-    block(local_states, 1)
-    send_states(1)
-    stage_d(2, 1)
-    stage_c(3)
-    block(scan_states, 0)
-    stage_e(2, 1)
-    send_prefixes(0)
-    stage_e(2, 0)
-    stage_f(2, 0)
-    block(scan_states, 1)
-    send_prefixes(1)
-    stage_d(3, 2)
-    stage_e(3, 2)
-    stage_f(2, 1)
-    block(query_piece, 0)
-    block(query_piece, 1)
-    stage_d(2, 2)
-    wait_prefixes(0)
-    stage_d(3, 1)
-    block(retention, 0, 0)
-    stage_e(2, 2)
-    stage_d(3, 0)
-    block(retention, 1, 0)
-    stage_f(3, 2)
-    wait_prefixes(1)
-    block(retention, 1, 1)
-    block(retention, 0, 1)
-    stage_e(3, 1)
-    stage_f(2, 2)
-    stage_f(3, 1)
-    wait_retained()
-    stage_e(3, 0)
-    block(out_piece, c, 0)
-    block(out_piece, other, 3)
-    block(out_piece, c, 2)
-    block(out_piece, c, 3)
-    stage_f(3, 0)
-    block(out_piece, other, 2)
-    block(out_piece, other, 0)
-    block(out_piece, c, 1)
-    block(out_piece, other, 1)
+    def wait_inputs():
+        for cp in in_copies:
+            cp.wait()
+
+    def send_rates():
+        rate_copy.start()
+
+    def wait_rates():
+        rate_copy.wait()
+
+    def send_normed(i):
+        norm_copy(i).start()
+
+    def wait_normed():
+        for i in range(4):
+            norm_copy(i).wait()
+
+    compute = (
+        norm, tables, decays, key_piece, query_piece, value_piece,
+        local_states, scan_states, retention, out_piece,
+    )
+
+    def run(step, *args):
+        with jax.named_scope(step.__name__ + "".join(f"_{a}" for a in args if isinstance(a, int))):
+            if step in compute:
+                pl.when(z < 4)(functools.partial(step, *args))
+            else:
+                step(*args)
+
+    run(stage_p, 0)
+    run(stage_p, 1)
+    run(stage_p, 2)
+    run(stage_p, 3)
+    run(send_rates)
+    run(stage_p, 4)
+    run(wait_inputs)
+    run(norm, 0)
+    run(stage_a, 0)
+    run(stage_a, 1)
+    run(stage_b, 0)
+    run(stage_a, 2)
+    run(stage_b, 1)
+    run(stage_c, 0)
+    run(norm, 1)
+    run(stage_a, 4)
+    run(stage_b, 2)
+    run(stage_c, 1)
+    run(stage_d, 1, 0)
+    run(norm, 2)
+    run(tables)
+    run(norm, 3)
+    run(send_normed, 3)
+    run(send_normed, 0)
+    run(stage_d, 0, 2)
+    run(stage_d, 0, 1)
+    run(wait_rates)
+    run(decays)
+    run(send_normed, 1)
+    run(stage_e, 0, 2)
+    run(stage_e, 1, 0)
+    run(stage_d, 1, 1)
+    run(stage_d, 1, 2)
+    run(stage_c, 2)
+    run(send_normed, 2)
+    run(wait_normed)
+    run(stage_f, 0, 2)
+    run(stage_e, 1, 1)
+    run(stage_f, 1, 0)
+    run(stage_b, 4)
+    run(stage_e, 0, 1)
+    run(stage_f, 0, 1)
+    run(stage_e, 1, 2)
+    run(key_piece, 0)
+    run(stage_d, 2, 0)
+    run(stage_d, 0, 0)
+    run(value_piece, 0)
+    run(stage_f, 1, 1)
+    run(value_piece, 1)
+    run(local_states, 0)
+    run(stage_f, 1, 2)
+    run(stage_e, 2, 0)
+    run(send_states, 0)
+    run(key_piece, 1)
+    run(value_piece, 2)
+    run(stage_a, 3)
+    run(stage_f, 2, 0)
+    run(value_piece, 3)
+    run(stage_d, 2, 2)
+    run(local_states, 1)
+    run(send_states, 1)
+    run(stage_d, 2, 1)
+    run(stage_c, 4)
+    run(scan_states, 0)
+    run(stage_e, 0, 0)
+    run(stage_b, 3)
+    run(send_prefixes, 0)
+    run(stage_e, 2, 1)
+    run(scan_states, 1)
+    run(stage_e, 2, 2)
+    run(stage_f, 0, 0)
+    run(stage_f, 2, 1)
+    run(send_prefixes, 1)
+    run(query_piece, 0)
+    run(stage_c, 3)
+    run(stage_f, 2, 2)
+    run(query_piece, 1)
+    run(wait_prefixes, 0)
+    run(retention, 1, 0)
+    run(stage_d, 4, 0)
+    run(retention, 0, 0)
+    run(wait_prefixes, 1)
+    run(stage_d, 3, 1)
+    run(retention, 1, 1)
+    run(stage_d, 3, 0)
+    run(stage_d, 3, 2)
+    run(retention, 0, 1)
+    run(stage_e, 4, 0)
+    run(stage_e, 3, 1)
+    run(wait_retained)
+    run(out_piece, c, 0)
+    run(stage_f, 4, 0)
+    run(stage_e, 3, 0)
+    run(out_piece, other, 0)
+    run(out_piece, c, 3)
+    run(stage_e, 3, 2)
+    run(stage_f, 3, 1)
+    run(out_piece, other, 3)
+    run(stage_f, 3, 2)
+    run(out_piece, c, 2)
+    run(stage_f, 3, 0)
+    run(out_piece, c, 1)
+    run(out_piece, other, 2)
+    run(out_piece, other, 1)
 
     for wave in range(WAVES):
         finish_sends(wave)
@@ -513,7 +560,8 @@
         drain(p_recv.at[half, pl.ds(0, SHARDS - 1)], ps.at[half])
     for h in range(4):
         drain(ret_send.at[0], rs.at[h])
-        drain(w.at[0], os.at[h])
+    for j in range(8):
+        drain(w.at[0], os.at[j])
 
 
 def body(tokens, norm_gain, w_query, w_key, w_value, w_out, decay_rate):
@@ -521,8 +569,8 @@
     any_spec = pl.BlockSpec(memory_space=pl.ANY)
     dma = pltpu.SemaphoreType.DMA
     scratch = [
-        pltpu.VMEM((16, 4, 4, 4, 32, 256), BF16),
-        pltpu.VMEM((12, 16, 256), BF16),
+        pltpu.VMEM((PIECES + 8, 4, 4, 4, 32, 128), BF16),
+        pltpu.VMEM((PIECES, 16, 128), BF16),
         pltpu.VMEM((LEN, D), BF16),
         pltpu.VMEM((2, LEN, D), BF16),
         pltpu.VMEM((1, D), F32),
@@ -547,7 +595,7 @@
         dma((4,)), dma((4,)), dma((WAVES,)), dma((WAVES,)), dma((WAVES,)), dma, dma, dma((4,)), dma((4,)),
         dma((WAVES,)), dma((WAVES,)), dma((WAVES,)), dma((WAVES,)), dma((WAVES,)), dma((WAVES,)),
         dma((WAVES,)), dma((WAVES, 3, 2, 2)), dma((WAVES, 3)), dma((WAVES, 3, 2)),
-        dma((2,)), dma((2,)), dma((2,)), dma((2,)), dma((4,)), dma((4,)), dma((4,)), dma((4,)),
+        dma((2,)), dma((2,)), dma((2,)), dma((2,)), dma((4,)), dma((4,)), dma((8,)), dma((8,)),
     ]
     args = (
         tokens, norm_gain[None], w_query, w_key, w_value, w_out, decay_rate[0],

time: 78.4 us -> 73.1 us (0.932)
  Pallas kernels: 77 us -> 71.6 us
    pallas_call x1, Pallas kernels: 77 us -> 71.6 us  [body(): pl.pallas_call(kernel, out_shape=jax.ShapeDtypeStruct((1, LEN, D), BF16),...]
where the time goes in v4:
time: 73.1 us; the launch traced here: 73 us
  Pallas kernels  71.6 us (98%)
  local copies, waits for them, and re-layouts  1.32 us (2%)
    pallas_call x1, Pallas kernels, body(): pl.pallas_call(kernel, out_shape=jax.ShapeDtypeStruct((1, LEN, D), BF16),...  71.6 us

profile of v4, /device:TPU:1, one launch (start us, length us, event | category | flops | bytes accessed | tf_op | source)
XLA Modules:
  0.0 73.0 jit_solution(748032299931674462)
XLA Ops:
  0.0 71.6 %shard_map.91 = bf16[1,512,2048]{2,1,0:T(8,128)(2,1)S(1)} custom-call(bf16[1,512,2048]{2,1,0:T(8,128)(2,1)} %tokens.1, f32[1,2048]{1,0:T(1,128)} %bitcast.2, bf16[16,1024]{1,0:T(8,128)(2,1)} %wq.1, bf16[16,1024]{1,0:T(8,128)(2,1)} %wk.1, bf16[16,2048]{1,0:T(8,128)(2,1)} %wv.1, bf16[16,2048]{1,0:T(8,128)(2,1)} %wo.1, f32[8,64]{1,0:T(8,128)} %bitcast.3, ...), custom_call_target="tpu_custom_call" | custom-call | tf_op jit(solution)/shard_map/pallas_call | solution.py:604
  71.6 1.3 %copy.11 = bf16[1,512,2048]{2,1,0:T(8,128)(2,1)} copy(bf16[1,512,2048]{2,1,0:T(8,128)(2,1)S(1)} %shard_map.91) | data formatting | bytes 4194304

commit v5 on v4

--- a/solution.py
+++ b/solution.py
@@ -25,11 +25,11 @@
 ROPE_BASE = 10000.0
 
 PLAN = (
-    (((1, 2, 0), "Q"), ((0, 1, 2), "K"), ((2, 0, 1), "V")),
-    (((2, 1, 0), "KV"), ((1, 0, 2), "VVV"), ((0, 2, 1), "KKV")),
-    (((2, 1, 0), "VV"), ((0, 2, 1), "Q"), ((1, 0, 2), "QQOO")),
+    (((1, 2, 0), "V"), ((0, 1, 2), "K"), ((2, 0, 1), "V")),
+    (((2, 1, 0), "KV"), ((1, 0, 2), "KKV"), ((0, 2, 1), "VV")),
+    (((2, 1, 0), "QQ"), ((0, 2, 1), "VV"), ((1, 0, 2), "QQOO")),
     (((2, 0, 1), "OO"), ((2, 1, 0), "O"), ((2, 1, 0), "O")),
-    (((0, 1, 2), "OO"), ((0, 2, 1), ""), ((2, 0, 1), "")),
+    (((0, 1, 2), "OO"), ((2, 1, 0), ""), ((1, 0, 2), "")),
 )
 WAVES = len(PLAN)
 PIECES = 24
@@ -108,7 +108,7 @@
     barrier = pltpu.get_barrier_semaphore()
     first_peers = [mate]
     for dim in range(3):
-        for step in (1, 3, 2):
+        for step in (2, 1, 3):
             first_peers += [device(dim, step), device(dim, step, other)]
     for dev in first_peers:
         pl.semaphore_signal(barrier, inc=1, device_id=dev, device_id_type=MESH)
@@ -119,12 +119,15 @@
         pltpu.make_async_copy(high_in.at[:, pl.ds(pl.multiple_of(shard * 16, 16), 16)], high, in_sem.at[2]),
         pltpu.make_async_copy(low_in, low, in_sem.at[3]),
     ]
-    for cp in in_copies + tok_copies:
-        cp.start()
     for wave, (first, count) in enumerate(WHOLE):
         for piece in range(first, first + count):
             pltpu.make_async_copy(columns_of(piece, c), w.at[piece, z, y, x, own_rows], own_sem.at[wave]).start()
             pltpu.make_async_copy(columns_of(piece, other), for_mate.at[piece], own_sem.at[wave]).start()
+        if wave == 0:
+            for cp in in_copies:
+                cp.start()
+    for cp in tok_copies:
+        cp.start()
     pl.semaphore_wait(barrier, len(first_peers))
     rate_copy = pltpu.make_async_remote_copy(
         rates_in, rates2, rate_s, rate_r, device_id=mate, device_id_type=MESH
@@ -169,35 +172,37 @@
             own = w.at[pieces, z, y, x, own_rows]
             theirs = for_mate.at[pieces]
             pltpu.make_async_remote_copy(
-                theirs, own, mate_s.at[wave], mate_r.at[wave], device_id=mate, device_id_type=MESH
+                theirs, own, mate_s.at[wave], mate_r.at[wave, part], device_id=mate, device_id_type=MESH
             ).start()
-            for step in (1, 3, 2):
+            for step in (2, 1, 3):
                 for src, core in ((own, c), (theirs, other)):
                     pltpu.make_async_remote_copy(
-                        src, own, p1s.at[wave], p1r.at[wave],
+                        src, own, p1s.at[wave], p1r.at[wave, part],
                         device_id=device(d1, step, core), device_id_type=MESH,
                     ).start()
 
     def stage_a(wave):
-        drain(mate_wait_ref(wave), mate_r.at[wave])
-        drain(p1_wait_ref(wave), p1r.at[wave])
         for part, (d1, d2, d3), first, count in parts_of(wave):
+            pieces = pl.ds(first, count)
+            drain(w.at[pieces, 0, 0, 0, pl.ds(0, 16)], mate_r.at[wave, part])
+            drain(w.at[pieces, 0, 0, pl.ds(0, 3)], p1r.at[wave, part])
             own = part_slice(first, count, {d2: here[d2], d3: here[d3]})
             for step in (1, 3):
-                send(own, p2s.at[wave], p2r.at[wave], device(d2, step))
+                send(own, p2s.at[wave], p2r.at[wave, part], device(d2, step))
 
     def stage_b(wave):
-        drain(p2_wait_ref(wave), p2r.at[wave])
         for part, (d1, d2, d3), first, count in parts_of(wave):
+            drain(w.at[pl.ds(first, count), pl.ds(0, 2), 0], p2r.at[wave, part])
             for i, step in enumerate((1, 3)):
                 origin = lax.rem(here[d2] + 4 - step, 4)
                 src = part_slice(first, count, {d1: HALF[i], d2: origin, d3: here[d3]})
-                send(src, p2fs.at[wave], p2fr.at[wave], device(d2, step))
+                send(src, p2fs.at[wave], p2fr.at[wave, part], device(d2, step))
 
     def stage_c(wave):
-        drain(p2f_wait_ref(wave), p2fr.at[wave])
         for sub in range(2):
             for part, (d1, d2, d3), first, count in parts_of(wave):
+                if sub == 0:
+                    drain(w.at[pl.ds(first, count), 0, 0], p2fr.at[wave, part])
                 for i, step in enumerate((1, 3)):
                     half = sub if i == 0 else 1 - sub
                     src = part_slice(first, count, {d2: HALF[half], d3: here[d3]})
@@ -452,90 +457,90 @@
     run(stage_p, 1)
     run(stage_p, 2)
     run(stage_p, 3)
-    run(send_rates)
     run(stage_p, 4)
-    run(wait_inputs)
-    run(norm, 0)
     run(stage_a, 0)
     run(stage_a, 1)
     run(stage_b, 0)
+    run(send_rates)
+    run(stage_a, 4)
+    run(wait_inputs)
+    run(norm, 0)
     run(stage_a, 2)
+    run(norm, 1)
     run(stage_b, 1)
+    run(norm, 2)
+    run(send_normed, 2)
     run(stage_c, 0)
-    run(norm, 1)
-    run(stage_a, 4)
     run(stage_b, 2)
+    run(send_normed, 1)
+    run(tables)
     run(stage_c, 1)
-    run(stage_d, 1, 0)
-    run(norm, 2)
-    run(tables)
-    run(norm, 3)
-    run(send_normed, 3)
     run(send_normed, 0)
     run(stage_d, 0, 2)
+    run(norm, 3)
+    run(stage_d, 1, 2)
     run(stage_d, 0, 1)
+    run(stage_e, 0, 2)
+    run(stage_d, 0, 0)
     run(wait_rates)
     run(decays)
-    run(send_normed, 1)
-    run(stage_e, 0, 2)
+    run(stage_d, 1, 0)
+    run(send_normed, 3)
+    run(wait_normed)
+    run(stage_e, 0, 0)
     run(stage_e, 1, 0)
     run(stage_d, 1, 1)
-    run(stage_d, 1, 2)
+    run(stage_e, 1, 2)
     run(stage_c, 2)
-    run(send_normed, 2)
-    run(wait_normed)
-    run(stage_f, 0, 2)
-    run(stage_e, 1, 1)
     run(stage_f, 1, 0)
-    run(stage_b, 4)
+    run(stage_f, 0, 0)
     run(stage_e, 0, 1)
     run(stage_f, 0, 1)
-    run(stage_e, 1, 2)
     run(key_piece, 0)
+    run(stage_f, 0, 2)
+    run(stage_d, 2, 1)
+    run(value_piece, 0)
     run(stage_d, 2, 0)
-    run(stage_d, 0, 0)
-    run(value_piece, 0)
+    run(stage_b, 4)
+    run(stage_e, 1, 1)
+    run(stage_f, 1, 2)
+    run(value_piece, 2)
+    run(stage_a, 3)
     run(stage_f, 1, 1)
     run(value_piece, 1)
     run(local_states, 0)
-    run(stage_f, 1, 2)
-    run(stage_e, 2, 0)
     run(send_states, 0)
     run(key_piece, 1)
-    run(value_piece, 2)
-    run(stage_a, 3)
-    run(stage_f, 2, 0)
+    run(stage_e, 2, 1)
+    run(stage_e, 2, 0)
+    run(stage_f, 2, 1)
     run(value_piece, 3)
     run(stage_d, 2, 2)
     run(local_states, 1)
+    run(stage_f, 2, 0)
     run(send_states, 1)
-    run(stage_d, 2, 1)
+    run(stage_b, 3)
+    run(scan_states, 0)
+    run(send_prefixes, 0)
+    run(scan_states, 1)
+    run(send_prefixes, 1)
     run(stage_c, 4)
-    run(scan_states, 0)
-    run(stage_e, 0, 0)
-    run(stage_b, 3)
-    run(send_prefixes, 0)
-    run(stage_e, 2, 1)
-    run(scan_states, 1)
+    run(query_piece, 0)
     run(stage_e, 2, 2)
-    run(stage_f, 0, 0)
-    run(stage_f, 2, 1)
-    run(send_prefixes, 1)
-    run(query_piece, 0)
     run(stage_c, 3)
     run(stage_f, 2, 2)
     run(query_piece, 1)
     run(wait_prefixes, 0)
     run(retention, 1, 0)
+    run(wait_prefixes, 1)
     run(stage_d, 4, 0)
-    run(retention, 0, 0)
-    run(wait_prefixes, 1)
-    run(stage_d, 3, 1)
     run(retention, 1, 1)
     run(stage_d, 3, 0)
     run(stage_d, 3, 2)
     run(retention, 0, 1)
     run(stage_e, 4, 0)
+    run(stage_d, 3, 1)
+    run(retention, 0, 0)
     run(stage_e, 3, 1)
     run(wait_retained)
     run(out_piece, c, 0)
@@ -544,11 +549,11 @@
     run(out_piece, other, 0)
     run(out_piece, c, 3)
     run(stage_e, 3, 2)
+    run(stage_f, 3, 2)
+    run(out_piece, other, 3)
     run(stage_f, 3, 1)
-    run(out_piece, other, 3)
-    run(stage_f, 3, 2)
+    run(stage_f, 3, 0)
     run(out_piece, c, 2)
-    run(stage_f, 3, 0)
     run(out_piece, c, 1)
     run(out_piece, other, 2)
     run(out_piece, other, 1)
@@ -592,8 +597,8 @@
         pltpu.VMEM((2, SHARDS, 32, DV), BF16),
         pltpu.VMEM((LEN, D), BF16),
         pltpu.VMEM((4, LEN, DV), BF16),
-        dma((4,)), dma((4,)), dma((WAVES,)), dma((WAVES,)), dma((WAVES,)), dma, dma, dma((4,)), dma((4,)),
-        dma((WAVES,)), dma((WAVES,)), dma((WAVES,)), dma((WAVES,)), dma((WAVES,)), dma((WAVES,)),
+        dma((4,)), dma((4,)), dma((WAVES,)), dma((WAVES,)), dma((WAVES, 3)), dma, dma, dma((4,)), dma((4,)),
+        dma((WAVES,)), dma((WAVES, 3)), dma((WAVES,)), dma((WAVES, 3)), dma((WAVES,)), dma((WAVES, 3)),
         dma((WAVES,)), dma((WAVES, 3, 2, 2)), dma((WAVES, 3)), dma((WAVES, 3, 2)),
         dma((2,)), dma((2,)), dma((2,)), dma((2,)), dma((4,)), dma((4,)), dma((8,)), dma((8,)),
     ]

time: 73.1 us -> 72.8 us (level)
  no operation moved by 1% of the time
where the time goes in v5:
time: 72.8 us; the launch traced here: 72.7 us
  Pallas kernels  71.3 us (98%)
  local copies, waits for them, and re-layouts  1.32 us (2%)
    pallas_call x1, Pallas kernels, body(): pl.pallas_call(kernel, out_shape=jax.ShapeDtypeStruct((1, LEN, D), BF16),...  71.3 us

profile of v5, /device:TPU:1, one launch (start us, length us, event | category | flops | bytes accessed | tf_op | source)
XLA Modules:
  0.0 72.7 jit_solution(14081982261523766290)
XLA Ops:
  0.0 71.3 %shard_map.91 = bf16[1,512,2048]{2,1,0:T(8,128)(2,1)S(1)} custom-call(bf16[1,512,2048]{2,1,0:T(8,128)(2,1)} %tokens.1, f32[1,2048]{1,0:T(1,128)} %bitcast.2, bf16[16,1024]{1,0:T(8,128)(2,1)} %wq.1, bf16[16,1024]{1,0:T(8,128)(2,1)} %wk.1, bf16[16,2048]{1,0:T(8,128)(2,1)} %wv.1, bf16[16,2048]{1,0:T(8,128)(2,1)} %wo.1, f32[8,64]{1,0:T(8,128)} %bitcast.3, ...), custom_call_target="tpu_custom_call" | custom-call | tf_op jit(solution)/shard_map/pallas_call | solution.py:609
  71.3 1.3 %copy.11 = bf16[1,512,2048]{2,1,0:T(8,128)(2,1)} copy(bf16[1,512,2048]{2,1,0:T(8,128)(2,1)S(1)} %shard_map.91) | data formatting | bytes 4194304

commit v6 on v5

--- a/solution.py
+++ b/solution.py
@@ -405,8 +405,8 @@
                         rs.at[h], rr.at[h], device_id=mate, device_id_type=MESH,
                     ).start()
 
-    def out_piece(core, j):
-        pieces = (2 * j, 2 * j + 1)
+    def out_piece(core, j, count=1):
+        pieces = range(2 * j, 2 * (j + count))
         if core is c:
             pieces = [AT["O"][i] for i in pieces]
         else:
@@ -415,7 +415,7 @@
             pieces = [PIECES + i for i in pieces]
         prod = jnp.dot(ret[...], pair(pieces), preferred_element_type=F32)
         at = pl.multiple_of(core * 1024 + j * 256, 256)
-        out[0, :, pl.ds(at, 256)] = prod.astype(BF16)
+        out[0, :, pl.ds(at, 256 * count)] = prod.astype(BF16)
 
     def wait_prefixes(half):
         drain(p_recv.at[half, pl.ds(0, SHARDS - 1)], pr.at[half])
@@ -553,10 +553,8 @@
     run(out_piece, other, 3)
     run(stage_f, 3, 1)
     run(stage_f, 3, 0)
-    run(out_piece, c, 2)
-    run(out_piece, c, 1)
-    run(out_piece, other, 2)
-    run(out_piece, other, 1)
+    run(out_piece, c, 1, 2)
+    run(out_piece, other, 1, 2)
 
     for wave in range(WAVES):
         finish_sends(wave)

time: 72.8 us -> 73 us (level)
  no operation moved by 1% of the time
where the time goes in v6:
time: 73 us; the launch traced here: 72.9 us
  Pallas kernels  71.5 us (98%)
  local copies, waits for them, and re-layouts  1.32 us (2%)
    pallas_call x1, Pallas kernels, body(): pl.pallas_call(kernel, out_shape=jax.ShapeDtypeStruct((1, LEN, D), BF16),...  71.5 us

profile of v6, /device:TPU:1, one launch (start us, length us, event | category | flops | bytes accessed | tf_op | source)
XLA Modules:
  0.0 72.9 jit_solution(17712145861863681771)
XLA Ops:
  0.0 71.5 %shard_map.91 = bf16[1,512,2048]{2,1,0:T(8,128)(2,1)S(1)} custom-call(bf16[1,512,2048]{2,1,0:T(8,128)(2,1)} %tokens.1, f32[1,2048]{1,0:T(1,128)} %bitcast.2, bf16[16,1024]{1,0:T(8,128)(2,1)} %wq.1, bf16[16,1024]{1,0:T(8,128)(2,1)} %wk.1, bf16[16,2048]{1,0:T(8,128)(2,1)} %wv.1, bf16[16,2048]{1,0:T(8,128)(2,1)} %wo.1, f32[8,64]{1,0:T(8,128)} %bitcast.3, ...), custom_call_target="tpu_custom_call" | custom-call | tf_op jit(solution)/shard_map/pallas_call | solution.py:607
  71.5 1.3 %copy.11 = bf16[1,512,2048]{2,1,0:T(8,128)(2,1)} copy(bf16[1,512,2048]{2,1,0:T(8,128)(2,1)S(1)} %shard_map.91) | data formatting | bytes 4194304
